TPU v7x, 256 devices: a whole 4x4x8 slice. The times are simulated.
256 devices in a mesh: sp: 64 (over z, x, core), tp: 4 (over y).
Axes of the slice: x: 4, y: 4, z: 8, core: 2. Of those that a mesh axis runs over, the one named last changes fastest.
Arguments:
- queries: bfloat16 [12288, 1536], P('sp', 'tp'), may hold values from -64 to 64
- latents: bfloat16 [12288, 512], P('sp'), may hold values from -6 to 6
- rope_key: bfloat16 [12288, 32], P('sp'), may hold values from -64 to 64
- w_key: bfloat16 [512, 1024], P(None, 'tp'), may hold values from -0.25 to 0.25
- w_value: bfloat16 [512, 1024], P(None, 'tp'), may hold values from -0.25 to 0.25
- w_out: bfloat16 [1024, 2048], P('tp'), may hold values from -0.59765625 to 0.59765625
- resid: bfloat16 [12288, 2048], P('sp', 'tp'), may hold values from -12 to 12
- gain_mix: float32 [2048], P('tp'), may hold values from 0.1 to 1.9
- w_gate: bfloat16 [2048, 3072], P('sp', 'tp'), may hold values from -0.125 to 0.125
- w_up: bfloat16 [2048, 3072], P('sp', 'tp'), may hold values from -0.125 to 0.125
- w_down: bfloat16 [3072, 2048], P('tp', 'sp'), may hold values from -0.41992188 to 0.41992188
- gain_out: float32 [2048], P('tp'), may hold values from 0.1 to 1.9
Outputs:
- layer_out: bfloat16 [12288, 2048], P('sp', 'tp')
All inputs are finite; a program needn't handle non-finite values.
Results may differ from a plain program's by a relative error of at most 0.014.
Values may be sent and summed in bfloat16 or wider, within the bound.
A program may use at most 128 MiB of HBM per device.

v0:
```python
import jax
import jax.numpy as jnp
from jax import lax
from jax.sharding import PartitionSpec as P

NOPE = 64
ROPE = 32
VDIM = 64
GRID_W = 64


ROTARY_BASE = 10000.0
NORM_EPSILON = 1e-06
DEEP_ALPHA = 8.0**0.25
HALF_STEP = 0.5


def from_everyone(x, axis):
    copies = jnp.broadcast_to(x, (lax.axis_size(axis), *x.shape))
    return lax.all_to_all(copies, axis, split_axis=0, concat_axis=0, tiled=True)


def of_everyone(x, axis):
    return from_everyone(x, axis).sum(axis=0)


def packed_total(arrays, axis):
    ends = [0]
    for a in arrays:
        ends.append(ends[-1] + a.size)
    total = of_everyone(jnp.concatenate([a.ravel() for a in arrays]), axis)
    return tuple((total[b:e].reshape(a.shape) for a, b, e in zip(arrays, ends, ends[1:])))


def side_by_side(arrays, axis, dim, along):
    widths = [a.shape[along] for a in arrays]
    both = jnp.concatenate(arrays, axis=along)
    filled = lax.all_gather(both, axis, axis=dim, tiled=True)
    return tuple(jnp.split(filled, [sum(widths[:k]) for k in range(1, len(widths))], axis=along))


def cut_along(x, dim, length):
    lengths = x.shape
    tiles = x.reshape(*lengths[:dim], length, lengths[dim] // length, *lengths[dim + 1 :])
    return jnp.moveaxis(tiles, dim, 0)


def sum_at_owner(x, axis, dim):
    length = lax.axis_size(axis)
    tiles = lax.all_to_all(cut_along(x, dim, length), axis, 0, 0, tiled=True)
    return jnp.sum(tiles.astype(jnp.float32), axis=0)


def joined_along(tiles, dim):
    tiles = jnp.moveaxis(tiles, 0, dim)
    lengths = tiles.shape
    return tiles.reshape(*lengths[:dim], lengths[dim] * lengths[dim + 1], *lengths[dim + 2 :])


def gather_directly(x, axis, dim):
    return joined_along(from_everyone(x, axis), dim)


def rotary_tables(positions, rotary_width, grid_width):
    grid_rows = (positions // grid_width).astype(jnp.float32)
    grid_cols = (positions % grid_width).astype(jnp.float32)
    freq_count = rotary_width // 4
    inverse = ROTARY_BASE ** (-jnp.arange(freq_count, dtype=jnp.float32) / freq_count)
    angle_table = jnp.concatenate(
        [grid_rows[:, None] * inverse, grid_cols[:, None] * inverse], axis=-1
    )
    return (jnp.cos(angle_table), jnp.sin(angle_table))


def rotate(vectors, cosine, sine):
    half_width = vectors.shape[-1] // 2
    leading = vectors[..., :half_width].astype(jnp.float32)
    trailing = vectors[..., half_width:].astype(jnp.float32)
    return jnp.concatenate(
        [leading * cosine - trailing * sine, leading * sine + trailing * cosine], axis=-1
    ).astype(jnp.bfloat16)


def attend_block(state, key_block, query_pair):
    maxima, totals, running = state
    key_nope, value_rows, key_rope = key_block
    q_nope, q_rope = query_pair
    head_count = q_nope.shape[1]
    rows_here = key_nope.shape[0]
    key_nope = key_nope.reshape(rows_here, head_count, -1)
    value_rows = value_rows.reshape(rows_here, head_count, -1)
    score_scale = (q_nope.shape[2] + q_rope.shape[2]) ** (-0.5)
    scores = jnp.einsum("qhd,khd->hqk", q_nope, key_nope, preferred_element_type=jnp.float32)
    scores = (
        scores + jnp.einsum("qhd,kd->hqk", q_rope, key_rope, preferred_element_type=jnp.float32)
    ) * score_scale
    new_max = jnp.maximum(maxima, jnp.max(scores, axis=-1))
    weights = jnp.exp(scores - new_max[:, :, None])
    factor = jnp.exp(maxima - new_max)
    totals = totals * factor + jnp.sum(weights, axis=-1)
    update = jnp.einsum(
        "hqk,khd->qhd", weights.astype(jnp.bfloat16), value_rows, preferred_element_type=jnp.float32
    )
    running = running * jnp.transpose(factor)[:, :, None] + update
    return (new_max, totals, running)


def block_length(length):
    block_rows = length
    while block_rows > 2048 and block_rows % 2 == 0:
        block_rows = block_rows // 2
    return block_rows


def fold_keys(state, pieces, query_pair):
    length = pieces[0].shape[0]
    block_rows = block_length(length)
    stacked = tuple(
        (member.reshape(length // block_rows, block_rows, member.shape[1]) for member in pieces)
    )

    def one_block(partial_value, key_block):
        return (attend_block(partial_value, key_block, query_pair), None)

    state, unused = lax.scan(one_block, state, stacked)
    return state


def split_norm(rows_in, gain_row):
    width_total = rows_in.shape[1] * lax.axis_size("tp")
    row_sums, squares = packed_total(
        (jnp.sum(rows_in, axis=1), jnp.sum(rows_in * rows_in, axis=1)), "tp"
    )
    row_mean = row_sums / width_total
    variance = squares / width_total - row_mean * row_mean
    return (
        (rows_in - row_mean[:, None]) * lax.rsqrt(variance + NORM_EPSILON)[:, None] * gain_row
    ).astype(jnp.bfloat16)


def local(
    queries,
    latents,
    rope_key,
    w_key,
    w_value,
    w_out,
    resid,
    gain_mix,
    w_gate,
    w_up,
    w_down,
    gain_out,
):
    local_rows = queries.shape[0]
    head_count = w_key.shape[1] // NOPE
    offset = lax.axis_index("sp") * local_rows
    positions = offset + jnp.arange(local_rows, dtype=jnp.int32)
    cosine, sine = rotary_tables(positions, ROPE, GRID_W)
    key_rot = rotate(rope_key, cosine, sine)
    shaped = queries.reshape(local_rows, head_count, NOPE + ROPE)
    q_nope = shaped[:, :, :NOPE]
    q_rot = rotate(shaped[:, :, NOPE:], cosine[:, None, :], sine[:, None, :])
    query_pair = (q_nope, q_rot)
    start_state = (
        jnp.full((head_count, local_rows), -jnp.inf, jnp.float32),
        jnp.zeros((head_count, local_rows), jnp.float32),
        jnp.zeros((local_rows, head_count, VDIM), jnp.float32),
    )
    key_nope = jnp.dot(latents, w_key, preferred_element_type=jnp.float32).astype(jnp.bfloat16)
    value_rows = jnp.dot(latents, w_value, preferred_element_type=jnp.float32).astype(jnp.bfloat16)
    state = fold_keys(
        start_state, side_by_side((key_nope, value_rows, key_rot), "sp", 0, 1), query_pair
    )
    maxima, totals, running = state
    heads_out = (
        (running / jnp.transpose(totals)[:, :, None])
        .reshape(local_rows, head_count * VDIM)
        .astype(jnp.bfloat16)
    )
    projected = jnp.dot(heads_out, w_out, preferred_element_type=jnp.float32)
    attn_cols = sum_at_owner(projected.astype(jnp.bfloat16), "tp", 1)
    hidden_in = split_norm(DEEP_ALPHA * resid.astype(jnp.float32) + attn_cols, gain_mix)
    whole_rows = gather_directly(hidden_in, "tp", 1)
    pieces = side_by_side((w_gate, w_up), "sp", 0, 1)
    gate_sum = jnp.dot(whole_rows, pieces[0], preferred_element_type=jnp.float32)
    up_sum = jnp.dot(whole_rows, pieces[1], preferred_element_type=jnp.float32)
    hidden = (jax.nn.silu(gate_sum) * up_sum).astype(jnp.bfloat16)
    down_terms = jnp.dot(
        hidden, lax.all_gather(w_down, "sp", axis=1, tiled=True), preferred_element_type=jnp.float32
    )
    mixer_cols = sum_at_owner(down_terms.astype(jnp.bfloat16), "tp", 1)
    return split_norm(DEEP_ALPHA * hidden_in.astype(jnp.float32) + HALF_STEP * mixer_cols, gain_out)


def solution(mesh):
    placed = (
        P("sp", "tp"),
        P("sp", None),
        P("sp", None),
        P(None, "tp"),
        P(None, "tp"),
        P("tp", None),
        P("sp", "tp"),
        P("tp"),
        P("sp", "tp"),
        P("sp", "tp"),
        P("tp", "sp"),
        P("tp"),
    )
    return jax.shard_map(
        local, mesh=mesh, in_specs=placed, out_specs=P("sp", "tp"), check_vma=False
    )
```

profile of v0, /device:TPU:1, one launch (start us, length us, event | category | flops | bytes accessed | tf_op | source)
XLA Modules:
  0.0 304.9 jit_solution(5436441630834050987)
XLA Ops:
  15.1 96.8 %all-gather.4.cloned.1.call-done = bf16[12288,544]{1,0:T(8,128)(2,1)} async-done(((bf16[192,544]{1,0:T(8,128)(2,1)}), bf16[12288,544]{1,0:T(8,128)(2,1)}) %all-gather.4.cloned.1.call-update) | async-done | bytes 13369360 | tf_op jit(solution)/shard_map/all_gather | solution.py:38
  111.9 3.2 %split.21 = bf16[12288,32]{1,0:T(8,128)(2,1)} slice(bf16[12288,544]{1,0:T(8,128)(2,1)} %all-gather.4.cloned.1.call-done), slice={[0:12288], [512:544]} | slice | bytes 1572864 | tf_op jit(solution)/shard_map/split | solution.py:39
  115.1 4.0 %copy.74 = bf16[8,1536,32]{1,2,0:T(8,128)(2,1)} copy(bf16[8,1536,32]{2,1,0:T(8,128)(2,1)} %bitcast.76) | data formatting | bytes 1572864
  119.1 10.1 %fusion.53 = (bf16[12288,256]{1,0:T(8,128)(2,1)}, bf16[12288,256]{1,0:T(8,128)(2,1)}) fusion(bf16[12288,544]{1,0:T(8,128)(2,1)} %all-gather.4.cloned.1.call-done), kind=kLoop, calls=%fused_computation.93 | loop fusion | bytes 25165824 | tf_op jit(solution)/shard_map/split | solution.py:39
  129.2 91.7 %while.15 = (s32[]{:T(128)}, f32[4,192]{1,0:T(4,128)S(1)}, f32[4,192]{1,0:T(4,128)S(1)}, f32[192,4,64]{0,2,1:T(8,128)}, bf16[8,1536,256]{2,1,0:T(8,128)(2,1)}, /...) while((s32[]{:T(128)}, f32[4,192]{1,0:T(4,128)S(1)}, ...), condition=%wide.region_3.4_spmd.clone, body=%wide.region_0.3_spmd.clone.sunk | while | flops 385896960 | bytes 52609740 | solution.py:125
  132.7 3.0 fusion.86
  136.0 3.5 %fusion.90 = f32[192,4,64]{0,2,1:T(8,128)S(1)} fusion(bf16[1536,4,64]{0,2,1:T(8,128)(2,1)S(1)} %bitcast.73, f32[4,192,1536]{2,1,0:T(8,128)} %get-tuple-element.247, f32[4,192]{1,0:T(4,128)S(1)} %get-tuple-element.273, f32[192,4,64]{0,2,1:T(8,128)S(1)} %copy-done.2, f32[192,4]{0,1:T(4,128)S(1)} %get-tuple-element.249, pred[]{:T(512)S(6)} %compare.14), kind=kOutput, calls=%fused_computation.8.clone.1 | convolution fusion | flops 153501696 | bytes 5904385 | tf_op jit(solution)/shard_map/while/body/eval_jaxpr/hqk,khd->qhd/dot_general | solution.py:101
  147.4 3.5 %fusion.90 = f32[192,4,64]{0,2,1:T(8,128)S(1)} fusion(bf16[1536,4,64]{0,2,1:T(8,128)(2,1)S(1)} %bitcast.73, f32[4,192,1536]{2,1,0:T(8,128)} %get-tuple-element.247, f32[4,192]{1,0:T(4,128)S(1)} %get-tuple-element.273, f32[192,4,64]{0,2,1:T(8,128)S(1)} %copy-done.2, f32[192,4]{0,1:T(4,128)S(1)} %get-tuple-element.249, pred[]{:T(512)S(6)} %compare.14), kind=kOutput, calls=%fused_computation.8.clone.1 | convolution fusion | flops 153501696 | bytes 5904385 | tf_op jit(solution)/shard_map/while/body/eval_jaxpr/hqk,khd->qhd/dot_general | solution.py:101
  158.8 3.7 %fusion.90 = f32[192,4,64]{0,2,1:T(8,128)S(1)} fusion(bf16[1536,4,64]{0,2,1:T(8,128)(2,1)S(1)} %bitcast.73, f32[4,192,1536]{2,1,0:T(8,128)} %get-tuple-element.247, f32[4,192]{1,0:T(4,128)S(1)} %get-tuple-element.273, f32[192,4,64]{0,2,1:T(8,128)S(1)} %copy-done.2, f32[192,4]{0,1:T(4,128)S(1)} %get-tuple-element.249, pred[]{:T(512)S(6)} %compare.14), kind=kOutput, calls=%fused_computation.8.clone.1 | convolution fusion | flops 153501696 | bytes 5904385 | tf_op jit(solution)/shard_map/while/body/eval_jaxpr/hqk,khd->qhd/dot_general | solution.py:101
  167.2 3.0 fusion.86
  170.5 3.5 %fusion.90 = f32[192,4,64]{0,2,1:T(8,128)S(1)} fusion(bf16[1536,4,64]{0,2,1:T(8,128)(2,1)S(1)} %bitcast.73, f32[4,192,1536]{2,1,0:T(8,128)} %get-tuple-element.247, f32[4,192]{1,0:T(4,128)S(1)} %get-tuple-element.273, f32[192,4,64]{0,2,1:T(8,128)S(1)} %copy-done.2, f32[192,4]{0,1:T(4,128)S(1)} %get-tuple-element.249, pred[]{:T(512)S(6)} %compare.14), kind=kOutput, calls=%fused_computation.8.clone.1 | convolution fusion | flops 153501696 | bytes 5904385 | tf_op jit(solution)/shard_map/while/body/eval_jaxpr/hqk,khd->qhd/dot_general | solution.py:101
  182.1 3.6 %fusion.90 = f32[192,4,64]{0,2,1:T(8,128)S(1)} fusion(bf16[1536,4,64]{0,2,1:T(8,128)(2,1)S(1)} %bitcast.73, f32[4,192,1536]{2,1,0:T(8,128)} %get-tuple-element.247, f32[4,192]{1,0:T(4,128)S(1)} %get-tuple-element.273, f32[192,4,64]{0,2,1:T(8,128)S(1)} %copy-done.2, f32[192,4]{0,1:T(4,128)S(1)} %get-tuple-element.249, pred[]{:T(512)S(6)} %compare.14), kind=kOutput, calls=%fused_computation.8.clone.1 | convolution fusion | flops 153501696 | bytes 5904385 | tf_op jit(solution)/shard_map/while/body/eval_jaxpr/hqk,khd->qhd/dot_general | solution.py:101
  193.6 3.5 %fusion.90 = f32[192,4,64]{0,2,1:T(8,128)S(1)} fusion(bf16[1536,4,64]{0,2,1:T(8,128)(2,1)S(1)} %bitcast.73, f32[4,192,1536]{2,1,0:T(8,128)} %get-tuple-element.247, f32[4,192]{1,0:T(4,128)S(1)} %get-tuple-element.273, f32[192,4,64]{0,2,1:T(8,128)S(1)} %copy-done.2, f32[192,4]{0,1:T(4,128)S(1)} %get-tuple-element.249, pred[]{:T(512)S(6)} %compare.14), kind=kOutput, calls=%fused_computation.8.clone.1 | convolution fusion | flops 153501696 | bytes 5904385 | tf_op jit(solution)/shard_map/while/body/eval_jaxpr/hqk,khd->qhd/dot_general | solution.py:101
  205.0 3.5 %fusion.90 = f32[192,4,64]{0,2,1:T(8,128)S(1)} fusion(bf16[1536,4,64]{0,2,1:T(8,128)(2,1)S(1)} %bitcast.73, f32[4,192,1536]{2,1,0:T(8,128)} %get-tuple-element.247, f32[4,192]{1,0:T(4,128)S(1)} %get-tuple-element.273, f32[192,4,64]{0,2,1:T(8,128)S(1)} %copy-done.2, f32[192,4]{0,1:T(4,128)S(1)} %get-tuple-element.249, pred[]{:T(512)S(6)} %compare.14), kind=kOutput, calls=%fused_computation.8.clone.1 | convolution fusion | flops 153501696 | bytes 5904385 | tf_op jit(solution)/shard_map/while/body/eval_jaxpr/hqk,khd->qhd/dot_general | solution.py:101
  213.0 3.0 fusion.86
  216.3 3.5 %fusion.90 = f32[192,4,64]{0,2,1:T(8,128)S(1)} fusion(bf16[1536,4,64]{0,2,1:T(8,128)(2,1)S(1)} %bitcast.73, f32[4,192,1536]{2,1,0:T(8,128)} %get-tuple-element.247, f32[4,192]{1,0:T(4,128)S(1)} %get-tuple-element.273, f32[192,4,64]{0,2,1:T(8,128)S(1)} %copy-done.2, f32[192,4]{0,1:T(4,128)S(1)} %get-tuple-element.249, pred[]{:T(512)S(6)} %compare.14), kind=kOutput, calls=%fused_computation.8.clone.1 | convolution fusion | flops 153501696 | bytes 5904385 | tf_op jit(solution)/shard_map/while/body/eval_jaxpr/hqk,khd->qhd/dot_general | solution.py:101
  222.4 15.8 %all_to_all.27 = bf16[4,192,512]{2,1,0:T(8,128)(2,1)S(1)} all-to-all(bf16[4,192,512]{2,1,0:T(8,128)(2,1)S(1)} %bitcast.77), channel_id=1, replica_groups=mesh['sp'=64,'tp'=4] {'tp'}, dimensions={0} | all-to-all | bytes 1572864 | tf_op jit(solution)/shard_map/all_to_all | solution.py:50
  238.7 6.6 %all_to_all.28 = f32[4,1,384]{2,1,0:T(1,128)S(1)} all-to-all(f32[4,1,384]{2,1,0:T(1,128)S(1)} %broadcast_in_dim.17), channel_id=1, replica_groups=mesh['sp'=64,'tp'=4] {'tp'}, dimensions={0} | all-to-all | bytes 12288 | tf_op jit(solution)/shard_map/all_to_all | solution.py:20
  245.6 12.4 %all_to_all.29 = bf16[4,192,512]{2,1,0:T(8,128)(2,1)S(1)} all-to-all(bf16[4,192,512]{2,1,0:T(8,128)(2,1)S(1)} %broadcast_in_dim.18), channel_id=1, replica_groups=mesh['sp'=64,'tp'=4] {'tp'}, dimensions={0} | all-to-all | bytes 1572864 | tf_op jit(solution)/shard_map/all_to_all | solution.py:20
  258.1 3.5 %fusion.20 = f32[192,768]{1,0:T(8,128)} fusion(bf16[192,2048]{1,0:T(8,128)(2,1)S(1)} %bitcast.81, bf16[2048,1536]{1,0:T(8,128)(2,1)} %all-gather.6.cloned.1.call-done), kind=kOutput, calls=%fused_computation.23 | convolution fusion | flops 603979776 | bytes 4521984 | tf_op jit(solution)/shard_map/dot_general | solution.py:186
  261.6 8.1 %all-gather.8.cloned.1.call-done = bf16[768,2048]{0,1:T(8,128)(2,1)} async-done(((bf16[768,32]{0,1:T(8,128)(2,1)}), bf16[768,2048]{0,1:T(8,128)(2,1)}) %all-gather.8.cloned.1.call-update) | async-done | bytes 3145744 | tf_op jit(solution)/shard_map/all_gather | solution.py:190
  269.7 5.2 %convolution_convert_fusion = bf16[192,2048]{1,0:T(8,128)(2,1)S(1)} fusion(bf16[768,2048]{0,1:T(8,128)(2,1)} %all-gather.8.cloned.1.call-done, bf16[192,2048]{1,0:T(8,128)(2,1)S(1)} %bitcast.82, bf16[2048,1536]{1,0:T(8,128)(2,1)} %all-gather.6.cloned.1.call-done, f32[192,768]{1,0:T(8,128)} %fusion.20), kind=kOutput, calls=%fused_computation.25 | convolution fusion | flops 1209237504 | bytes 8454144 | tf_op jit(solution)/shard_map/dot_general | solution.py:189
  274.9 15.6 %all_to_all.30 = bf16[4,192,512]{2,1,0:T(8,128)(2,1)S(1)} all-to-all(bf16[4,192,512]{2,1,0:T(8,128)(2,1)S(1)} %bitcast.79), channel_id=1, replica_groups=mesh['sp'=64,'tp'=4] {'tp'}, dimensions={0} | all-to-all | bytes 1572864 | tf_op jit(solution)/shard_map/all_to_all | solution.py:50
  290.9 6.5 %all_to_all.31 = f32[4,1,384]{2,1,0:T(1,128)S(1)} all-to-all(f32[4,1,384]{2,1,0:T(1,128)S(1)} %broadcast_in_dim.19), channel_id=1, replica_groups=mesh['sp'=64,'tp'=4] {'tp'}, dimensions={0} | all-to-all | bytes 12288 | tf_op jit(solution)/shard_map/all_to_all | solution.py:20
  (169 shorter events, 66.1 us)
Async XLA Ops:
  6.5 215.4 %copy-start = (bf16[256,2048]{1,0:T(8,128)(2,1)S(1)}, bf16[256,2048]{1,0:T(8,128)(2,1)}, u32[]{:S(2)}) copy-start(bf16[256,2048]{1,0:T(8,128)(2,1)} %param.19) | copy-start | bytes 3145732
  6.5 105.4 %all-gather.4.cloned.1.call-start = ((), (), s32[]{:S(2)}) async-start(), calls=%async_computation.5 | async-start | bytes 15974400 | tf_op jit(solution)/shard_map/all_gather | solution.py:38
  11.1 247.0 %all-gather.6.cloned.1.call-start = ((), (), s32[]{:S(2)}) async-start(), calls=%async_computation.6 | async-start | bytes 6389760 | tf_op jit(solution)/shard_map/all_gather | solution.py:38
  12.7 257.0 %all-gather.8.cloned.1.call-start = ((), (), s32[]{:S(2)}) async-start(), calls=%async_computation.7 | async-start | bytes 3194880 | tf_op jit(solution)/shard_map/all_gather | solution.py:190
  132.7 3.3 %copy-start.2 = (f32[192,4,64]{0,2,1:T(8,128)S(1)}, f32[192,4,64]{0,2,1:T(8,128)}, u32[]{:S(2)}) copy-start(f32[192,4,64]{0,2,1:T(8,128)} %get-tuple-element.264) | copy-start | bytes 589828 | tf_op jit(solution)/shard_map/while
  136.0 3.8 %copy-start.1 = (f32[4,192,1536]{2,1,0:T(8,128)S(1)}, f32[4,192,1536]{2,1,0:T(8,128)}, u32[]{:S(2)}) copy-start(f32[4,192,1536]{2,1,0:T(8,128)} %get-tuple-element.247) | copy-start | bytes 14155780 | tf_op jit(solution)/shard_map/while
  144.1 3.3 %copy-start.2 = (f32[192,4,64]{0,2,1:T(8,128)S(1)}, f32[192,4,64]{0,2,1:T(8,128)}, u32[]{:S(2)}) copy-start(f32[192,4,64]{0,2,1:T(8,128)} %get-tuple-element.264) | copy-start | bytes 589828 | tf_op jit(solution)/shard_map/while
  147.4 3.8 %copy-start.1 = (f32[4,192,1536]{2,1,0:T(8,128)S(1)}, f32[4,192,1536]{2,1,0:T(8,128)}, u32[]{:S(2)}) copy-start(f32[4,192,1536]{2,1,0:T(8,128)} %get-tuple-element.247) | copy-start | bytes 14155780 | tf_op jit(solution)/shard_map/while
  155.5 3.3 %copy-start.2 = (f32[192,4,64]{0,2,1:T(8,128)S(1)}, f32[192,4,64]{0,2,1:T(8,128)}, u32[]{:S(2)}) copy-start(f32[192,4,64]{0,2,1:T(8,128)} %get-tuple-element.264) | copy-start | bytes 589828 | tf_op jit(solution)/shard_map/while
  158.7 4.1 %copy-start.1 = (f32[4,192,1536]{2,1,0:T(8,128)S(1)}, f32[4,192,1536]{2,1,0:T(8,128)}, u32[]{:S(2)}) copy-start(f32[4,192,1536]{2,1,0:T(8,128)} %get-tuple-element.247) | copy-start | bytes 14155780 | tf_op jit(solution)/shard_map/while
  167.2 3.3 %copy-start.2 = (f32[192,4,64]{0,2,1:T(8,128)S(1)}, f32[192,4,64]{0,2,1:T(8,128)}, u32[]{:S(2)}) copy-start(f32[192,4,64]{0,2,1:T(8,128)} %get-tuple-element.264) | copy-start | bytes 589828 | tf_op jit(solution)/shard_map/while
  170.5 3.9 %copy-start.1 = (f32[4,192,1536]{2,1,0:T(8,128)S(1)}, f32[4,192,1536]{2,1,0:T(8,128)}, u32[]{:S(2)}) copy-start(f32[4,192,1536]{2,1,0:T(8,128)} %get-tuple-element.247) | copy-start | bytes 14155780 | tf_op jit(solution)/shard_map/while
  178.8 3.3 %copy-start.2 = (f32[192,4,64]{0,2,1:T(8,128)S(1)}, f32[192,4,64]{0,2,1:T(8,128)}, u32[]{:S(2)}) copy-start(f32[192,4,64]{0,2,1:T(8,128)} %get-tuple-element.264) | copy-start | bytes 589828 | tf_op jit(solution)/shard_map/while
  182.0 3.9 %copy-start.1 = (f32[4,192,1536]{2,1,0:T(8,128)S(1)}, f32[4,192,1536]{2,1,0:T(8,128)}, u32[]{:S(2)}) copy-start(f32[4,192,1536]{2,1,0:T(8,128)} %get-tuple-element.247) | copy-start | bytes 14155780 | tf_op jit(solution)/shard_map/while
  186.0 0.8 copy-start.3
  190.3 3.3 %copy-start.2 = (f32[192,4,64]{0,2,1:T(8,128)S(1)}, f32[192,4,64]{0,2,1:T(8,128)}, u32[]{:S(2)}) copy-start(f32[192,4,64]{0,2,1:T(8,128)} %get-tuple-element.264) | copy-start | bytes 589828 | tf_op jit(solution)/shard_map/while
  193.6 3.8 %copy-start.1 = (f32[4,192,1536]{2,1,0:T(8,128)S(1)}, f32[4,192,1536]{2,1,0:T(8,128)}, u32[]{:S(2)}) copy-start(f32[4,192,1536]{2,1,0:T(8,128)} %get-tuple-element.247) | copy-start | bytes 14155780 | tf_op jit(solution)/shard_map/while
  201.7 3.3 %copy-start.2 = (f32[192,4,64]{0,2,1:T(8,128)S(1)}, f32[192,4,64]{0,2,1:T(8,128)}, u32[]{:S(2)}) copy-start(f32[192,4,64]{0,2,1:T(8,128)} %get-tuple-element.264) | copy-start | bytes 589828 | tf_op jit(solution)/shard_map/while
  204.9 3.8 %copy-start.1 = (f32[4,192,1536]{2,1,0:T(8,128)S(1)}, f32[4,192,1536]{2,1,0:T(8,128)}, u32[]{:S(2)}) copy-start(f32[4,192,1536]{2,1,0:T(8,128)} %get-tuple-element.247) | copy-start | bytes 14155780 | tf_op jit(solution)/shard_map/while
  213.0 3.3 %copy-start.2 = (f32[192,4,64]{0,2,1:T(8,128)S(1)}, f32[192,4,64]{0,2,1:T(8,128)}, u32[]{:S(2)}) copy-start(f32[192,4,64]{0,2,1:T(8,128)} %get-tuple-element.264) | copy-start | bytes 589828 | tf_op jit(solution)/shard_map/while
  216.3 3.8 %copy-start.1 = (f32[4,192,1536]{2,1,0:T(8,128)S(1)}, f32[4,192,1536]{2,1,0:T(8,128)}, u32[]{:S(2)}) copy-start(f32[4,192,1536]{2,1,0:T(8,128)} %get-tuple-element.247) | copy-start | bytes 14155780 | tf_op jit(solution)/shard_map/while
  220.9 17.5 %copy-start.4 = (bf16[192,512]{1,0:T(8,128)(2,1)S(1)}, bf16[192,512]{1,0:T(8,128)(2,1)}, u32[]{:S(2)}) copy-start(bf16[192,512]{1,0:T(8,128)(2,1)} %param.20) | copy-start | bytes 589828
  220.9 24.4 %copy-start.5 = (f32[512]{0:T(512)S(1)}, f32[512]{0:T(512)}, u32[]{:S(2)}) copy-start(f32[512]{0:T(512)} %param.21) | copy-start | bytes 6148
  274.8 22.7 %copy-start.6 = (f32[512]{0:T(512)S(1)}, f32[512]{0:T(512)}, u32[]{:S(2)}) copy-start(f32[512]{0:T(512)} %param.25) | copy-start | bytes 6148
  (7 other events, 5.7 us)
Sparse Core Ops, SparseCore 0:
  11.2 100.6 all-gather.3
  114.7 77.5 all-gather.5
  195.0 74.6 all-gather.7
where the time goes:
time: 306 us; the launch traced here: 305 us
  waiting for transfers between devices  106 us (35%)
  matrix products  77.3 us (25%)
  blocking collectives  56.9 us (19%)
  local copies, waits for them, and re-layouts  37.8 us (12%)
  other arithmetic  13.3 us (4%)
  between operations  13.3 us (4%)
    all_gather x2, waiting for transfers between devices, side_by_side(): filled = lax.all_gather(both, axis, axis=dim, tiled=True)  96.8 us
    all_to_all x2, blocking collectives, sum_at_owner(): tiles = lax.all_to_all(cut_along(x, dim, length), axis, 0, 0, tiled=True)  31.5 us
    dot_general x8, matrix products, attend_block(): jnp.einsum('hqk,khd->qhd', weights.astype(jnp.bfloat16), value_rows, pref...  28.1 us
    all_to_all x3, blocking collectives, from_everyone(): return lax.all_to_all(copies, axis, split_axis=0, concat_axis=0, tiled=True)  25.5 us
    dot_general x8, matrix products, attend_block(): jnp.einsum('qhd,khd->hqk', q_nope, key_nope, preferred_element_type=jnp.f...  23.8 us
    dynamic_slice x24, local copies, waits for them, and re-layouts, fold_keys(): state, unused = lax.scan(one_block, state, stacked)  16.2 us
    dot_general x8, matrix products, attend_block(): jnp.einsum('qhd,kd->hqk', q_rope, key_rope, preferred_element_type=jnp.fl...  13.8 us
    split x2, local copies, waits for them, and re-layouts, side_by_side(): jnp.split(filled, [sum(widths[:k]) for k in range(1, len(widths))], axis=...  13.3 us
  transfers between devices with their start and end apart: 3, of which 2 were waited for; matrix products, arithmetic and copies ran while one was open for 38% of the time, Pallas kernels for 0%

commit v1 on v0

v1 whole, which is shorter than its diff:
```python
import jax
import jax.numpy as jnp
from jax import lax
from jax.experimental import pallas as pl
from jax.experimental.pallas import tpu as pltpu
from jax.sharding import PartitionSpec as P

MESH = pl.DeviceIdType.MESH
F32 = jnp.float32
BF = jnp.bfloat16

HD = 64
ROPE = 32
GRID_W = 64
ROTARY_BASE = 10000.0
EPS = 1e-06
ALPHA = 8.0**0.25
HALF = 0.5
NZ, NX, NY = 8, 4, 4
T = 192
TQ = 48
NQ = 768
QB = 256
D = 2048
FC = 768
SCALE = (1.4426950408889634) * (96.0**-0.5)


class Ring:
    def __init__(self, n, pos, dev, blk, half, sems, log):
        self.n, self.pos, self.dev = n, pos, dev
        self.blk, self.half, self.sems, self.log = blk, half, sems, log

    def at(self, k):
        return lax.rem(self.pos + (k + 2 * self.n), self.n)

    def copy(self, ref, d, t):
        ss, rs = self.sems[d]
        return pltpu.make_async_remote_copy(
            src_ref=ref,
            dst_ref=ref,
            send_sem=ss.at[t],
            recv_sem=rs.at[t],
            device_id=self.dev(self.at(1 if d == 0 else -1)),
            device_id_type=MESH,
        )

    def send(self, ref, d, t):
        cp = self.copy(ref, d, t)
        cp.start()
        self.log.append(cp)

    def start(self):
        for d in (0, 1):
            self.send(self.blk(self.pos), d, 0)

    def arrived(self, d, t):
        return self.at(-t if d == 0 else t)

    def step(self, t):
        last = self.n // 2
        for d in (0, 1):
            p = self.arrived(d, t)
            if t < last:
                self.copy(self.blk(p), d, t - 1).wait_recv()
                self.send(self.blk(p) if t < last - 1 else self.half(p, d), d, t)
            else:
                self.copy(self.half(p, d), d, t - 1).wait_recv()


def kernel(
    q_ref, lat_ref, rk_ref, wk_ref, wv_ref, wo_ref, res_ref, gm_ref, wg_ref, wu_ref, wd_ref, go_ref, cs_ref, sn_ref,
    out_ref,
    kvsend, qsend, kvr, qin, rhs, kvt, sbuf, pbuf, obuf, mbuf, osend, hb, wo, resb, gsend, gains,
    wgu, wdt, hid, mixed, part, prec, outs, orec,
    s_kvx, r_kvx, s_qx, r_qx, s_res, r_res, s_g, r_g,
    s_zkv, r_zkv, s_dkv, r_dkv, s_zgu, r_zgu, s_xgu, r_xgu, s_dgu, r_dgu,
    s_xwd, r_xwd, s_zwd, r_zwd, s_dwd, r_dwd, s_ywo, r_ywo, s_dwo, r_dwo,
    s_o, r_o, s_yh, r_yh, s_p, r_p, s_f, r_f,
):
    sp = lax.axis_index("sp")
    y = lax.axis_index("tp")
    c = lax.rem(sp, 2)
    x = lax.rem(sp // 2, NX)
    z = sp // (2 * NX)
    log = []

    def dev(zz, xx, cc, yy):
        return ((zz * NX + xx) * 2 + cc, yy)

    def mod4(v):
        return lax.rem(v + 8, 4)

    partner = dev(z, x, 1 - c, y)

    def rcopy(src, dst, ss, rs, to):
        return pltpu.make_async_remote_copy(
            src_ref=src, dst_ref=dst, send_sem=ss, recv_sem=rs, device_id=to, device_id_type=MESH
        )

    def go(cp):
        cp.start()
        log.append(cp)

    def come(ref, ss, rs):
        rcopy(ref, ref, ss, rs, partner).wait_recv()

    barrier = pltpu.get_barrier_semaphore()
    peers = [dev(z, mod4(x + dx), c, mod4(y + dy)) for dx in range(4) for dy in range(4) if dx or dy]
    peers += [dev(lax.rem(z + 1, NZ), x, c, y), dev(lax.rem(z + NZ - 1, NZ), x, c, y), partner]
    for peer in peers:
        pl.semaphore_signal(barrier, inc=1, device_id=peer, device_id_type=MESH)

    cs, sn = cs_ref[...], sn_ref[...]

    def rotated(t):
        swapped = jnp.concatenate([t[:, ROPE // 2 :], t[:, : ROPE // 2]], axis=1)
        return t * cs + swapped * sn

    lat = lat_ref[...]
    k = jnp.dot(lat, wk_ref[...], preferred_element_type=F32)
    v = jnp.dot(lat, wv_ref[...], preferred_element_type=F32)
    kr = rotated(rk_ref[...].astype(F32))
    krp = jnp.concatenate([kr[TQ * i : TQ * i + TQ] for i in range(4)], axis=1).astype(BF)
    for h in range(4):
        kv = jnp.concatenate([k[:, HD * h : HD * h + HD], v[:, HD * h : HD * h + HD]], axis=1).astype(BF)
        for i in range(4):
            kvsend[h, i] = kv[TQ * i : TQ * i + TQ]
        kvsend[h, 4] = krp
    q = q_ref[...].astype(F32)
    for h in range(4):
        qh = q[:, 96 * h : 96 * h + 96]
        full = jnp.concatenate([qh[:, :HD], rotated(qh[:, HD:]), jnp.zeros((T, 32), F32)], axis=1)
        qsend[h] = full.astype(BF)
    gsend[0] = gm_ref[...]
    gsend[1] = go_ref[...]
    wgu[0, z, x, c] = wg_ref[...]
    wgu[1, z, x, c] = wu_ref[...]
    wdt[z, x, c] = jnp.transpose(wd_ref[...].astype(F32)).astype(BF)
    wo[y] = wo_ref[...]

    pl.semaphore_wait(barrier, len(peers))

    for dx in range(1, 4):
        xt = mod4(x + dx)
        to = dev(z, xt, c, y)
        go(rcopy(kvsend.at[xt], kvr.at[z, c, :, pl.ds(TQ * x, TQ), :], s_kvx.at[dx - 1], r_kvx.at[dx - 1], to))
    for dx in range(1, 4):
        xt = mod4(x + dx)
        to = dev(z, xt, c, y)
        go(rcopy(qsend.at[xt], qin.at[x], s_qx.at[dx - 1], r_qx.at[dx - 1], to))
    kvr[z, c, :, pl.ds(pl.multiple_of(TQ * x, 16), TQ), :] = kvsend[x]
    qin[x] = qsend[x]

    zdev = lambda p: dev(p, x, c, y)
    xdev = lambda p: dev(z, p, c, y)
    ydev = lambda p: dev(z, x, c, p)
    ring_kv = Ring(
        NZ, z, zdev,
        lambda p: kvr.at[p, c],
        lambda p, h: kvr.at[p, c, :, pl.ds(96 * h, 96), :],
        [(s_zkv.at[0], r_zkv.at[0]), (s_zkv.at[1], r_zkv.at[1])], log,
    )
    ring_gu = Ring(
        NZ, z, zdev,
        lambda p: wgu.at[:, p, x, c],
        lambda p, h: wgu.at[:, p, x, c, pl.ds(16 * h, 16), :],
        [(s_zgu.at[0], r_zgu.at[0]), (s_zgu.at[1], r_zgu.at[1])], log,
    )
    ring_wd = Ring(
        NX, x, xdev,
        lambda p: wdt.at[z, p, c],
        lambda p, h: wdt.at[z, p, c, pl.ds(16 * h, 16), :],
        [(s_xwd.at[0], r_xwd.at[0]), (s_xwd.at[1], r_xwd.at[1])], log,
    )
    ring_wdz = Ring(
        NZ, z, zdev,
        lambda p: wdt.at[p, :, c],
        lambda p, h: wdt.at[p, pl.ds(2 * h, 2), c],
        [(s_zwd.at[0], r_zwd.at[0]), (s_zwd.at[1], r_zwd.at[1])], log,
    )
    ring_wo = Ring(
        NY, y, ydev,
        lambda p: wo.at[p, pl.ds(pl.multiple_of(128 * c, 128), 128), :],
        lambda p, h: wo.at[p, pl.ds(pl.multiple_of(128 * c + 64 * h, 64), 64), :],
        [(s_ywo.at[0], r_ywo.at[0]), (s_ywo.at[1], r_ywo.at[1])], log,
    )

    def gu_ring(k):
        p = lax.rem(z + k + NZ, NZ)
        return Ring(
            NX, x, xdev,
            lambda q: wgu.at[:, p, q, c],
            lambda q, h: wgu.at[:, p, q, c, pl.ds(16 * h, 16), :],
            [(s_xgu.at[k % NZ, 0], r_xgu.at[k % NZ, 0]), (s_xgu.at[k % NZ, 1], r_xgu.at[k % NZ, 1])], log,
        )

    xrings = {k: gu_ring(k) for k in (0, -1, 1, -2, 2, -3, 3, 4)}

    def to_partner(ref, ss, rs):
        go(rcopy(ref, ref, ss, rs, partner))

    from_partner = come

    def zk(k):
        return lax.rem(z + k + NZ, NZ)

    ring_gu.start()
    ring_wd.start()
    xrings[0].start()

    for dy in range(1, 4):
        yt = mod4(y + dy)
        to = dev(z, x, c, yt)
        go(rcopy(res_ref.at[pl.ds(pl.multiple_of(TQ * yt, 16), TQ), :], resb.at[y], s_res.at[dy - 1], r_res.at[dy - 1], to))
        go(rcopy(gsend, gains.at[y], s_g.at[dy - 1], r_g.at[dy - 1], to))
    resb[y] = res_ref[pl.ds(pl.multiple_of(TQ * y, 16), TQ), :]
    gains[y] = gsend[...]
    ring_wo.start()

    for dx in range(1, 4):
        xf = mod4(x - dx)
        come(kvr.at[z, c, :, pl.ds(TQ * xf, TQ), :], s_kvx.at[dx - 1], r_kvx.at[dx - 1])
    ring_kv.start()

    def kv_out(k):
        to_partner(kvr.at[zk(k), c], s_dkv.at[k % NZ], r_dkv.at[k % NZ])

    def kv_in(k):
        from_partner(kvr.at[zk(k), 1 - c], s_dkv.at[k % NZ], r_dkv.at[k % NZ])

    kv_out(0)

    kvt[...] = jnp.ones_like(kvt)
    obuf[...] = jnp.zeros_like(obuf)
    mbuf[...] = jnp.full_like(mbuf, -1e30)
    for dx in range(1, 4):
        xf = mod4(x - dx)
        come(qin.at[xf], s_qx.at[dx - 1], r_qx.at[dx - 1])
    rhs[...] = jnp.zeros_like(rhs)
    qt = jnp.transpose(qin[...].reshape(NQ, 128).astype(F32)).astype(BF)
    for i in range(4):
        rhs[i, 0:HD] = qt[0:HD]
        rhs[i, 128 + 32 * i : 160 + 32 * i] = qt[HD : HD + 32]

    def attend(p):
        for cc in range(2):
            t = jnp.transpose(kvr[p, cc, 0:4].reshape(NQ, 128).astype(F32))
            kvt[cc, HD:128] = t[HD:128].astype(BF)

        def one(qb, carry):
            qs = pl.ds(pl.multiple_of(qb * QB, QB), QB)
            mx = None
            for cc in range(2):
                krb = kvr[p, cc, 4]
                for i in range(4):
                    lhs = jnp.concatenate([kvr[p, cc, i], krb], axis=1)
                    s = jnp.dot(lhs, rhs[i, :, qs], preferred_element_type=F32)
                    r = (cc * 4 + i) * T
                    sbuf[r : r + T] = s
                    part_max = jnp.max(s.reshape(T // 8, 8, QB), axis=0)
                    mx = part_max if mx is None else jnp.maximum(mx, part_max)
            m_old = mbuf[0:1, qs]
            m_new = jnp.maximum(m_old, jnp.max(mx, axis=0, keepdims=True))
            mbuf[0:1, qs] = m_new
            factor = jnp.exp2((m_old - m_new) * SCALE)
            shift = m_new * SCALE
            acc = None
            for cc in range(2):
                for i in range(4):
                    r = (cc * 4 + i) * T
                    pbuf[r : r + T] = jnp.exp2(sbuf[r : r + T] * SCALE - shift).astype(BF)
                got = jnp.dot(kvt[cc], pbuf[cc * NQ : cc * NQ + NQ], preferred_element_type=F32)
                acc = got if acc is None else acc + got
            obuf[:, qs] = obuf[:, qs] * factor + acc
            return carry

        lax.fori_loop(0, NQ // QB, one, 0)

    def gu_out(k):
        to_partner(wgu.at[:, zk(k), :, c], s_dgu.at[k % NZ], r_dgu.at[k % NZ])

    def gu_in(k):
        from_partner(wgu.at[:, zk(k), :, 1 - c], s_dgu.at[k % NZ], r_dgu.at[k % NZ])

    def wd_out(k):
        to_partner(wdt.at[zk(k), :, c], s_dwd.at[k % NZ], r_dwd.at[k % NZ])

    def wd_in(k):
        from_partner(wdt.at[zk(k), :, 1 - c], s_dwd.at[k % NZ], r_dwd.at[k % NZ])

    def wo_out(k):
        to_partner(ring_wo.blk(ring_wo.at(k)), s_dwo.at[k % NY - 1], r_dwo.at[k % NY - 1])

    def wo_in(k):
        p = ring_wo.at(k)
        ref = wo.at[p, pl.ds(pl.multiple_of(128 - 128 * c, 128), 128), :]
        from_partner(ref, s_dwo.at[k % NY - 1], r_dwo.at[k % NY - 1])

    ring_wd.step(1)
    kv_in(0)
    attend(z)
    for t in range(1, 5):
        ks = (-t, t) if t < 4 else (4,)
        ring_kv.step(t)
        for kk in ks:
            kv_out(kk)
        ring_gu.step(t)
        for kk in ks:
            xrings[kk].start()
        if t == 1:
            ring_wd.step(2)
            xrings[0].step(1)
        if t == 2:
            xrings[0].step(2)
            gu_out(0)
            xrings[-1].step(1)
            xrings[1].step(1)
            ring_wo.step(1)
            wo_out(-1)
            wo_out(1)
        if t == 3:
            xrings[-1].step(2)
            gu_out(-1)
            xrings[1].step(2)
            gu_out(1)
            xrings[-2].step(1)
            xrings[2].step(1)
        if t == 4:
            xrings[-2].step(2)
            gu_out(-2)
            xrings[2].step(2)
            gu_out(2)
            xrings[-3].step(1)
            xrings[3].step(1)
            ring_wo.step(2)
            wo_out(2)
            ring_wdz.start()
            wd_out(0)
        for kk in ks:
            kv_in(kk)
            attend(zk(kk))

    par = lax.rem(x, 2)
    on = obuf[HD:128] / obuf[0:1]
    par_f = par.astype(F32)
    full = jnp.concatenate([on * (1.0 - par_f), on * par_f], axis=0)
    osend[...] = jnp.transpose(full).astype(BF).reshape(4, T, 128)
    for dx in range(4):
        for dy in range(4):
            if dx or dy:
                xt, yt = mod4(x + dx), mod4(y + dy)
                n = dx * 4 + dy - 1
                src = osend.at[xt, pl.ds(pl.multiple_of(TQ * yt, 16), TQ), :]
                go(rcopy(src, hb.at[4 * y + x], s_o.at[n], r_o.at[n], dev(z, xt, c, yt)))
    hb[4 * y + x] = osend[x, pl.ds(pl.multiple_of(TQ * y, 16), TQ), :]
    xrings[-3].step(2)
    gu_out(-3)
    xrings[3].step(2)
    gu_out(3)
    xrings[4].step(1)
    ring_wdz.step(1)
    wd_out(-1)
    wd_out(1)
    for kk in (-1, 1, 2):
        wo_in(kk)
    for dy in range(1, 4):
        yf = mod4(y - dy)
        come(resb.at[yf], s_res.at[dy - 1], r_res.at[dy - 1])
        come(gains.at[yf], s_g.at[dy - 1], r_g.at[dy - 1])
    for dx in range(4):
        for dy in range(4):
            if dx or dy:
                n = dx * 4 + dy - 1
                slot = 4 * mod4(y - dy) + mod4(x - dx)
                come(hb.at[slot], s_o.at[n], r_o.at[n])

    def gain(n):
        return jnp.concatenate([gains[g, n] for g in range(4)], axis=1)

    def normed(rows, gain_row):
        mean = jnp.sum(rows, axis=1, keepdims=True) * (1.0 / D)
        var = jnp.sum(rows * rows, axis=1, keepdims=True) * (1.0 / D) - mean * mean
        return ((rows - mean) * lax.rsqrt(var + EPS) * gain_row).astype(BF)

    attn = None
    for g in range(4):
        pairs = [hb[4 * g + 2 * j] + hb[4 * g + 2 * j + 1] for j in range(2)]
        term = jnp.dot(jnp.concatenate(pairs, axis=1), wo[g], preferred_element_type=F32)
        term = term.astype(BF).astype(F32)
        attn = term if attn is None else attn + term
    res = jnp.concatenate([resb[g] for g in range(4)], axis=1).astype(F32)
    hid[y] = normed(ALPHA * res + attn, gain(0))

    ring_h = Ring(
        NY, y, ydev,
        lambda p: hid.at[p],
        lambda p, h: hid.at[p, :, pl.ds(1024 * h, 1024)],
        [(s_yh.at[0], r_yh.at[0]), (s_yh.at[1], r_yh.at[1])], log,
    )
    ring_h.start()
    xrings[4].step(2)
    gu_out(4)
    ring_wdz.step(2)
    wd_out(-2)
    wd_out(2)
    ring_h.step(1)
    for kk in (0, -1, 1, -2, 2, -3, 3, 4):
        gu_in(kk)
    ring_wdz.step(3)
    wd_out(-3)
    wd_out(3)
    ring_h.step(2)

    rows = hid[...].reshape(T, D)

    def gate_up(j, carry):
        cols = pl.ds(pl.multiple_of(j * QB, QB), QB)
        gate = jnp.dot(rows, wgu[0, :, :, :, :, cols].reshape(D, QB), preferred_element_type=F32)
        up = jnp.dot(rows, wgu[1, :, :, :, :, cols].reshape(D, QB), preferred_element_type=F32)
        mixed[:, cols] = (gate / (1.0 + jnp.exp(-gate)) * up).astype(BF)
        return carry

    lax.fori_loop(0, FC // QB, gate_up, 0)
    ring_wdz.step(4)
    wd_out(4)
    for kk in (0, -1, 1, -2, 2, -3, 3, 4):
        wd_in(kk)
    units = mixed[...]

    def down(j, carry):
        w = wdt[j].reshape(QB, FC)
        got = lax.dot_general(units, w, (((1,), (1,)), ((), ())), preferred_element_type=F32)
        part[:, :, pl.ds(pl.multiple_of(j * QB, QB), QB)] = got.astype(BF).reshape(4, TQ, QB)
        return carry

    lax.fori_loop(0, NZ, down, 0)
    for dy in range(1, 4):
        yt = mod4(y + dy)
        go(rcopy(part.at[yt], prec.at[dy - 1], s_p.at[dy - 1], r_p.at[dy - 1], dev(z, x, c, yt)))
    total = part[y].astype(F32)
    for dy in range(1, 4):
        come(prec.at[dy - 1], s_p.at[dy - 1], r_p.at[dy - 1])
        total = total + prec[dy - 1].astype(F32)
    outs[...] = normed(ALPHA * hid[y].astype(F32) + HALF * total, gain(1))
    for dy in range(1, 4):
        yt = mod4(y + dy)
        src = outs.at[:, pl.ds(pl.multiple_of(512 * yt, 512), 512)]
        go(rcopy(src, orec.at[y], s_f.at[dy - 1], r_f.at[dy - 1], dev(z, x, c, yt)))
    orec[y] = outs[:, pl.ds(pl.multiple_of(512 * y, 512), 512)]
    for dy in range(1, 4):
        yf = mod4(y - dy)
        come(orec.at[yf], s_f.at[dy - 1], r_f.at[dy - 1])
    out_ref[...] = orec[...].reshape(T, 512)
    for cp in log:
        cp.wait_send()


def local(queries, latents, rope_key, w_key, w_value, w_out, resid, gain_mix, w_gate, w_up, w_down, gain_out):
    start = lax.axis_index("sp") * T
    positions = start + jnp.arange(T, dtype=jnp.int32)
    grid_rows = (positions // GRID_W).astype(F32)
    grid_cols = (positions % GRID_W).astype(F32)
    count = ROPE // 4
    inverse = ROTARY_BASE ** (-jnp.arange(count, dtype=F32) / count)
    angles = jnp.concatenate([grid_rows[:, None] * inverse, grid_cols[:, None] * inverse], axis=-1)
    cos, sin = jnp.cos(angles), jnp.sin(angles)
    cs = jnp.concatenate([cos, cos], axis=1)
    sn = jnp.concatenate([-sin, sin], axis=1)
    dma = pltpu.SemaphoreType.DMA
    V = pltpu.VMEM

    def pair(*shape):
        return [dma(shape), dma(shape)]

    sems = []
    for shape in (
        (3,), (3,), (3,), (3,),
        (2, 4), (8,), (2, 4), (8, 2, 2), (8,),
        (2, 2), (2, 4), (8,), (2, 2), (3,),
        (15,), (2, 2), (3,), (3,),
    ):
        sems += pair(*shape)
    scratch = [
        V((4, 5, TQ, 128), BF),
        V((4, T, 128), BF),
        V((NZ, 2, 5, T, 128), BF),
        V((4, T, 128), BF),
        V((4, 256, NQ), BF),
        V((2, 128, NQ), BF),
        V((8 * T, QB), F32),
        V((8 * T, QB), BF),
        V((128, NQ), F32),
        V((8, NQ), F32),
        V((4, T, 128), BF),
        V((16, TQ, 128), BF),
        V((NY, 256, D), BF),
        V((NY, TQ, 512), BF),
        V((2, 1, 512), F32),
        V((NY, 2, 1, 512), F32),
        V((2, NZ, NX, 2, 32, FC), BF),
        V((NZ, NX, 2, 32, FC), BF),
        V((NY, TQ, D), BF),
        V((T, FC), BF),
        V((NY, TQ, D), BF),
        V((3, TQ, D), BF),
        V((TQ, D), BF),
        V((NY, TQ, 512), BF),
    ]
    vm = pl.BlockSpec(memory_space=pltpu.VMEM)
    return pl.pallas_call(
        kernel,
        out_shape=jax.ShapeDtypeStruct((T, 512), BF),
        in_specs=[vm] * 14,
        out_specs=vm,
        scratch_shapes=scratch + sems,
        compiler_params=pltpu.CompilerParams(
            collective_id=0, has_side_effects=True, vmem_limit_bytes=60 * 1024 * 1024
        ),
    )(
        queries, latents, rope_key, w_key, w_value, w_out, resid, gain_mix.reshape(1, 512),
        w_gate, w_up, w_down, gain_out.reshape(1, 512), cs, sn,
    )


def solution(mesh):
    placed = (
        P("sp", "tp"), P("sp", None), P("sp", None), P(None, "tp"), P(None, "tp"), P("tp", None),
        P("sp", "tp"), P("tp"), P("sp", "tp"), P("sp", "tp"), P("tp", "sp"), P("tp"),
    )
    return jax.shard_map(local, mesh=mesh, in_specs=placed, out_specs=P("sp", "tp"), check_vma=False)
```

time: 306 us -> 101 us (0.33)
  waiting for transfers between devices: 106 us -> 0 us
  Pallas kernels: 0 us -> 94.8 us
  matrix products: 77.3 us -> 0 us
  blocking collectives: 56.9 us -> 0 us
  local copies, waits for them, and re-layouts: 37.8 us -> 5.38 us
  between operations: 13.3 us -> 0.04 us
  other arithmetic: 13.3 us -> 0.19 us
    all_gather x3 -> x0, waiting for transfers between devices: 105 us -> none  [the longest x2 96.8 us: side_by_side(): filled = lax.all_gather(both, axis, axis=dim, tiled=True)]
    pallas_call x0 -> x1, Pallas kernels: none -> 94.8 us  [local(): pl.pallas_call(kernel, out_shape=jax.ShapeDtypeStruct((T, 512), BF), in_s...]
    dot_general x29 -> x0, matrix products: 77.3 us -> none  [the longest x8 28.1 us: attend_block(): jnp.einsum('hqk,khd->qhd', weights.astype(jnp.bfloat16), value_rows, pref...]
    all_to_all x5 -> x0, blocking collectives: 56.9 us -> none  [the longest x2 31.5 us: sum_at_owner(): tiles = lax.all_to_all(cut_along(x, dim, length), axis, 0, 0, tiled=True)]
    dynamic_slice x24 -> x0, local copies, waits for them, and re-layouts: 16.2 us -> none  [fold_keys(): state, unused = lax.scan(one_block, state, stacked)]
    split x2 -> x0, local copies, waits for them, and re-layouts: 13.3 us -> none  [side_by_side(): jnp.split(filled, [sum(widths[:k]) for k in range(1, len(widths))], axis=...]
    reduce_sum x14 -> x0, other arithmetic: 6.88 us -> none  [the longest x8 6.25 us: attend_block(): totals = totals * factor + jnp.sum(weights, axis=-1)]
  transfers between devices with their start and end apart: 3 -> 0, of which waited for: 2 -> 0; matrix products, arithmetic and copies ran while one was open for 38% -> 0% of each run, Pallas kernels for 0% -> 0%
where the time goes in v1:
time: 101 us; the launch traced here: 100 us
  Pallas kernels  94.8 us (94%)
  local copies, waits for them, and re-layouts  5.38 us (5%)
    pallas_call x1, Pallas kernels, local(): pl.pallas_call(kernel, out_shape=jax.ShapeDtypeStruct((T, 512), BF), in_s...  94.8 us
    unnamed x7, local copies, waits for them, and re-layouts  3.9 us

profile of v1, /device:TPU:1, one launch (start us, length us, event | category | flops | bytes accessed | tf_op | source)
XLA Modules:
  0.0 100.4 jit_solution(17406840667476651382)
XLA Ops:
  0.0 0.1 broadcast_multiply_fusion.1
  0.1 0.1 fusion.5
  0.2 0.0 copy-start.1
  0.2 0.7 copy-done.1
  0.9 0.7 copy.15.rk_ref
  1.6 0.7 copy.17.cs_ref
  2.4 0.0 copy-start
  2.4 0.7 copy.18.sn_ref
  3.1 0.1 copy-done
  3.2 0.8 copy.16.wd_ref
  4.0 94.8 %shard_map.118 = bf16[192,512]{1,0:T(8,128)(2,1)} custom-call(bf16[192,384]{1,0:T(8,128)(2,1)} %q_ref.1, bf16[192,512]{1,0:T(8,128)(2,1)} %lat_ref.1, bf16[192,32]{1,0:T(8,128)(2,1)} %copy.15.rk_ref, bf16[512,256]{1,0:T(8,128)(2,1)} %wk_ref.1, bf16[512,256]{1,0:T(8,128)(2,1)} %wv_ref.1, bf16[256,2048]{1,0:T(8,128)(2,1)} %wo_ref.1, bf16[192,512]{1,0:T(8,128)(2,1)} %res_ref.1, ...), custom_call_target="tpu_custom_call" | custom-call | tf_op jit(solution)/shard_map/pallas_call | solution.py:511
  98.8 1.6 %copy.20 = bf16[192,512]{1,0:T(8,128)(2,1)} copy(bf16[192,512]{1,0:T(8,128)(2,1)} %shard_map.118) | data formatting | bytes 393216
  (4 shorter events, 0.0 us)
Async XLA Ops:
  0.2 0.7 copy-start.1
  2.4 0.8 copy-start

commit v2 on v1

v2 whole, which is shorter than its diff:
```python
import jax
import jax.numpy as jnp
from jax import lax
from jax.experimental import pallas as pl
from jax.experimental.pallas import tpu as pltpu
from jax.sharding import PartitionSpec as P

MESH = pl.DeviceIdType.MESH
F32 = jnp.float32
BF = jnp.bfloat16

HD = 64
ROPE = 32
GRID_W = 64
ROTARY_BASE = 10000.0
EPS = 1e-06
ALPHA = 8.0**0.25
HALF = 0.5
NZ, NX, NY = 8, 4, 4
T = 192
TQ = 48
NQ = 768
QB = 256
D = 2048
FC = 768
SCALE = (1.4426950408889634) * (96.0**-0.5)


class Ring:
    def __init__(self, n, pos, dev, blk, half, sems, log, pieces=False):
        self.n, self.pos, self.dev, self.pieces = n, pos, dev, pieces
        self.blk, self.half, self.sems, self.log = blk, half, sems, log

    def at(self, k):
        return lax.rem(self.pos + (k + 2 * self.n), self.n)

    def copy(self, p, d, t, h):
        ss, rs = self.sems[d]
        ref = self.blk(p) if h is None else self.half(p, h)
        at = (t, h) if self.pieces else (t,)
        return pltpu.make_async_remote_copy(
            src_ref=ref,
            dst_ref=ref,
            send_sem=ss.at[at],
            recv_sem=rs.at[at],
            device_id=self.dev(self.at(1 if d == 0 else -1)),
            device_id_type=MESH,
        )

    def parts(self, t):
        if t == self.n // 2 - 1:
            return ((0, 0), (1, 1))
        if self.pieces:
            return ((0, 0), (1, 1), (0, 1), (1, 0))
        return ((0, None), (1, None))

    def send(self, p, d, t, h):
        cp = self.copy(p, d, t, h)
        cp.start()
        self.log.append(cp)

    def start(self):
        for d, h in self.parts(0):
            self.send(self.pos, d, 0, h)

    def arrived(self, d, t):
        return self.at(-t if d == 0 else t)

    def take(self, t):
        for d, h in self.parts(t - 1):
            self.copy(self.arrived(d, t), d, t - 1, h).wait_recv()

    def pass_on(self, t):
        for d, h in self.parts(t):
            self.send(self.arrived(d, t), d, t, h)

    def step(self, t):
        for d, h in self.parts(t - 1):
            p = self.arrived(d, t)
            self.copy(p, d, t - 1, h).wait_recv()
            if self.pieces and t < self.n // 2 and (d, h) in self.parts(t):
                self.send(p, d, t, h)
        if not self.pieces and t < self.n // 2:
            self.pass_on(t)


def kernel(
    q_ref, lat_ref, rk_ref, wk_ref, wv_ref, wo_ref, res_ref, gm_ref, wg_ref, wu_ref, wd_ref, go_ref, cs_ref, sn_ref,
    out_ref,
    kvsend, qsend, kvr, qin, qt, kp, kvt, sbuf, pbuf, obuf, mbuf, osend, hb, wo, resb, gains,
    wgu, wdt, hid, mixed, part, crec, stat,
    s_kvx, r_kvx, s_qx, r_qx, s_res, r_res, s_g, r_g,
    s_zkv, r_zkv, s_dkv, r_dkv, s_zgu, r_zgu, s_xgu, r_xgu, s_dgu, r_dgu,
    s_xwd, r_xwd, s_zwd, r_zwd, s_dwd, r_dwd, s_ywo, r_ywo, s_dwo, r_dwo,
    s_o, r_o, s_yh, r_yh, s_p, r_p, s_f, r_f,
):
    sp = lax.axis_index("sp")
    y = lax.axis_index("tp")
    c = lax.rem(sp, 2)
    x = lax.rem(sp // 2, NX)
    z = sp // (2 * NX)
    log = []

    def dev(zz, xx, cc, yy):
        return ((zz * NX + xx) * 2 + cc, yy)

    def mod4(v):
        return lax.rem(v + 8, 4)

    def zk(k):
        return lax.rem(z + k + NZ, NZ)

    partner = dev(z, x, 1 - c, y)

    def rcopy(src, dst, ss, rs, to):
        return pltpu.make_async_remote_copy(
            src_ref=src, dst_ref=dst, send_sem=ss, recv_sem=rs, device_id=to, device_id_type=MESH
        )

    def go(cp):
        cp.start()
        log.append(cp)

    def come(ref, ss, rs):
        rcopy(ref, ref, ss, rs, partner).wait_recv()

    def to_partner(ref, ss, rs):
        go(rcopy(ref, ref, ss, rs, partner))

    def rows48(i):
        return pl.ds(pl.multiple_of(TQ * i, 16), TQ)

    def cols512(i):
        return pl.ds(pl.multiple_of(512 * i, 512), 512)

    barrier = pltpu.get_barrier_semaphore()
    peers = [dev(z, mod4(x + dx), c, mod4(y + dy)) for dx in range(4) for dy in range(4) if dx or dy]
    peers += [dev(zk(1), x, c, y), dev(zk(-1), x, c, y), partner]
    for peer in peers:
        pl.semaphore_signal(barrier, inc=1, device_id=peer, device_id_type=MESH)

    wgu[0, z, x, c] = wg_ref[...]
    wgu[1, z, x, c] = wu_ref[...]
    wdt[z, x, c] = wd_ref[...]
    wo[y] = wo_ref[...]
    gains[y, 0] = gm_ref[...]
    gains[y, 1] = go_ref[...]
    lat = lat_ref[...]
    k = jnp.dot(lat, wk_ref[...], preferred_element_type=F32)
    v = jnp.dot(lat, wv_ref[...], preferred_element_type=F32)
    cst, snt, rkt = cs_ref[...], sn_ref[...], rk_ref[...].astype(F32)
    swapped = jnp.concatenate([rkt[ROPE // 2 :], rkt[: ROPE // 2]], axis=0)
    krt = rkt * cst + swapped * snt
    table = jnp.transpose(jnp.concatenate([cst, snt, krt, krt], axis=0))
    kr = table[:, 2 * ROPE : 3 * ROPE]
    krp = jnp.concatenate([kr[TQ * i : TQ * i + TQ] for i in range(4)], axis=1).astype(BF)
    for h in range(4):
        kv = jnp.concatenate([k[:, HD * h : HD * h + HD], v[:, HD * h : HD * h + HD]], axis=1).astype(BF)
        for i in range(4):
            kvsend[h, i] = kv[TQ * i : TQ * i + TQ]
        kvsend[h, 4] = krp

    zdev = lambda p: dev(p, x, c, y)
    xdev = lambda p: dev(z, p, c, y)
    ydev = lambda p: dev(z, x, c, p)

    def pairs(ss, rs):
        return [(ss.at[d], rs.at[d]) for d in (0, 1)]

    ring_kv = Ring(
        NZ, z, zdev,
        lambda p: kvr.at[p, c],
        lambda p, h: kvr.at[p, c, :, pl.ds(96 * h, 96), :],
        pairs(s_zkv, r_zkv), log, pieces=True,
    )
    ring_gu = Ring(
        NZ, z, zdev,
        lambda p: wgu.at[:, p, x, c],
        lambda p, h: wgu.at[:, p, x, c, pl.ds(16 * h, 16), :],
        pairs(s_zgu, r_zgu), log,
    )
    ring_wd = Ring(
        NX, x, xdev,
        lambda p: wdt.at[z, p, c],
        lambda p, h: wdt.at[z, p, c, pl.ds(16 * h, 16), :],
        pairs(s_xwd, r_xwd), log,
    )
    ring_wdz = Ring(
        NZ, z, zdev,
        lambda p: wdt.at[p, :, c],
        lambda p, h: wdt.at[p, pl.ds(2 * h, 2), c],
        pairs(s_zwd, r_zwd), log,
    )
    ring_wo = Ring(
        NY, y, ydev,
        lambda p: wo.at[p, pl.ds(pl.multiple_of(128 * c, 128), 128), :],
        lambda p, h: wo.at[p, pl.ds(pl.multiple_of(128 * c + 64 * h, 64), 64), :],
        pairs(s_ywo, r_ywo), log,
    )
    ring_h = Ring(
        NY, y, ydev,
        lambda p: hid.at[p],
        lambda p, h: hid.at[p, :, pl.ds(1024 * h, 1024)],
        pairs(s_yh, r_yh), log, pieces=True,
    )

    def gu_ring(k):
        p = zk(k)
        return Ring(
            NX, x, xdev,
            lambda q: wgu.at[:, p, q, c],
            lambda q, h: wgu.at[:, p, q, c, pl.ds(16 * h, 16), :],
            [(s_xgu.at[k % NZ, d], r_xgu.at[k % NZ, d]) for d in (0, 1)], log,
        )

    xr = {k: gu_ring(k) for k in (0, -1, 1, -2, 2, -3, 3, 4)}

    def kv_out(k):
        to_partner(kvr.at[zk(k), c], s_dkv.at[k % NZ], r_dkv.at[k % NZ])

    def kv_in(k):
        come(kvr.at[zk(k), 1 - c], s_dkv.at[k % NZ], r_dkv.at[k % NZ])

    def gu_out(k):
        to_partner(wgu.at[:, zk(k), :, c], s_dgu.at[k % NZ], r_dgu.at[k % NZ])

    def gu_in(k):
        come(wgu.at[:, zk(k), :, 1 - c], s_dgu.at[k % NZ], r_dgu.at[k % NZ])

    def wd_out(k):
        to_partner(wdt.at[zk(k), :, c], s_dwd.at[k % NZ], r_dwd.at[k % NZ])

    def wd_in(k):
        come(wdt.at[zk(k), :, 1 - c], s_dwd.at[k % NZ], r_dwd.at[k % NZ])

    def wo_out(k):
        to_partner(ring_wo.blk(ring_wo.at(k)), s_dwo.at[k % NY - 1], r_dwo.at[k % NY - 1])

    def wo_in(k):
        ref = wo.at[ring_wo.at(k), pl.ds(pl.multiple_of(128 - 128 * c, 128), 128), :]
        come(ref, s_dwo.at[k % NY - 1], r_dwo.at[k % NY - 1])

    pl.semaphore_wait(barrier, len(peers))

    ring_gu.start()
    for dx in (1, 3, 2):
        xt = mod4(x + dx)
        go(rcopy(kvsend.at[xt], kvr.at[z, c, :, rows48(x), :], s_kvx.at[dx - 1], r_kvx.at[dx - 1], xdev(xt)))
    kvr[z, c, :, rows48(x), :] = kvsend[x]
    cs, sn = table[:, :ROPE], table[:, ROPE : 2 * ROPE]
    q = q_ref[...].astype(F32)
    for h in range(4):
        qr = q[:, 96 * h + HD : 96 * h + 96]
        turned = qr * cs + jnp.concatenate([qr[:, ROPE // 2 :], qr[:, : ROPE // 2]], axis=1) * sn
        full = jnp.concatenate([q[:, 96 * h : 96 * h + HD], turned, jnp.zeros((T, 32), F32)], axis=1)
        qsend[h] = full.astype(BF)
    for dx in (1, 3, 2):
        xt = mod4(x + dx)
        go(rcopy(qsend.at[xt], qin.at[x], s_qx.at[dx - 1], r_qx.at[dx - 1], xdev(xt)))
    qin[x] = qsend[x]
    xr[0].start()
    ring_wd.start()

    for dy in (1, 3, 2):
        yt = mod4(y + dy)
        go(rcopy(res_ref.at[rows48(yt), :], resb.at[y], s_res.at[dy - 1], r_res.at[dy - 1], ydev(yt)))
        go(rcopy(gains.at[y], gains.at[y], s_g.at[dy - 1], r_g.at[dy - 1], ydev(yt)))
    resb[y] = res_ref[rows48(y), :]
    ring_wo.start()

    ring_gu.step(1)
    for dx in (1, 3, 2):
        come(kvr.at[z, c, :, rows48(mod4(x - dx)), :], s_kvx.at[dx - 1], r_kvx.at[dx - 1])
    ring_kv.start()
    kv_out(0)
    xr[-1].start()
    xr[1].start()

    kvt[...] = jnp.ones_like(kvt)
    obuf[...] = jnp.zeros_like(obuf)
    mbuf[...] = jnp.full_like(mbuf, -1e30)
    for dx in (1, 3, 2):
        come(qin.at[mod4(x - dx)], s_qx.at[dx - 1], r_qx.at[dx - 1])
    qt[...] = jnp.transpose(qin[...].reshape(NQ, 128))

    def attend(p):
        for cc in range(2):
            kr = kvr[p, cc, 4]
            for i in range(4):
                lo = (cc * 4 + i) * T
                kp[lo : lo + T] = jnp.concatenate(
                    [kvr[p, cc, i][:, :HD], kr[:, ROPE * i : ROPE * i + ROPE], jnp.zeros((T, ROPE), BF)], axis=1
                )
            kvt[cc, HD:128] = jnp.transpose(kvr[p, cc, 0:4].reshape(NQ, 128))[HD:128]

        def scores(qb, j):
            s = jnp.dot(kp[T * j : T * j + T], qt[:, QB * qb : QB * qb + QB], preferred_element_type=F32)
            sbuf[qb % 2, T * j : T * j + T] = s
            return jnp.max(s.reshape(T // 8, 8, QB), axis=0)

        maxima = [scores(0, j) for j in range(8)]
        for qb in range(3):
            qs = slice(QB * qb, QB * qb + QB)
            b = qb % 2
            top = maxima[0]
            for other in maxima[1:]:
                top = jnp.maximum(top, other)
            m_old = mbuf[0:1, qs]
            m_new = jnp.maximum(m_old, jnp.max(top, axis=0, keepdims=True))
            mbuf[0:1, qs] = m_new
            factor = jnp.exp2((m_old - m_new) * SCALE)
            shift = m_new * SCALE
            maxima = []
            acc = None
            for j in range(8):
                if qb < 2:
                    maxima.append(scores(qb + 1, j))
                pbuf[b, T * j : T * j + T] = jnp.exp2(sbuf[b, T * j : T * j + T] * SCALE - shift).astype(BF)
                if j % 4 == 3:
                    cc = j // 4
                    got = jnp.dot(kvt[cc], pbuf[b, cc * NQ : cc * NQ + NQ], preferred_element_type=F32)
                    acc = got if acc is None else acc + got
            obuf[:, qs] = obuf[:, qs] * factor + acc

    kv_in(0)
    attend(z)
    ring_kv.step(1)
    kv_out(-1)
    kv_out(1)
    xr[0].step(1)
    ring_wd.step(1)
    kv_in(-1)
    attend(zk(-1))
    kv_in(1)
    attend(zk(1))
    ring_kv.step(2)
    kv_out(-2)
    kv_out(2)
    xr[0].step(2)
    gu_out(0)
    ring_wd.step(2)
    wd_out(0)
    xr[-1].step(1)
    xr[1].step(1)
    ring_gu.take(2)
    xr[-2].start()
    xr[2].start()
    kv_in(-2)
    attend(zk(-2))
    kv_in(2)
    attend(zk(2))
    ring_kv.step(3)
    kv_out(-3)
    kv_out(3)
    ring_gu.pass_on(2)
    ring_wdz.start()
    xr[-1].step(2)
    gu_out(-1)
    xr[1].step(2)
    gu_out(1)
    ring_wo.step(1)
    wo_out(-1)
    wo_out(1)
    kv_in(-3)
    attend(zk(-3))
    ring_kv.step(4)
    kv_out(4)
    xr[-2].step(1)
    xr[2].step(1)
    kv_in(3)
    attend(zk(3))
    kv_in(4)
    attend(zk(4))

    par = lax.rem(x, 2).astype(F32)
    on = obuf[HD:128] / obuf[0:1]
    full = jnp.concatenate([on * (1.0 - par), on * par], axis=0)
    osend[...] = jnp.transpose(full).astype(BF).reshape(4, T, 128)
    others = [(dx, dy) for dx in range(4) for dy in range(4) if dx or dy]
    for dx, dy in sorted(others, key=lambda o: -(min(o[0], 4 - o[0]) + min(o[1], 4 - o[1]))):
        xt, yt = mod4(x + dx), mod4(y + dy)
        n = dx * 4 + dy - 1
        go(rcopy(osend.at[xt, rows48(yt), :], hb.at[4 * y + x], s_o.at[n], r_o.at[n], dev(z, xt, c, yt)))
    hb[4 * y + x] = osend[x, rows48(y), :]
    ring_gu.step(3)
    xr[-3].start()
    xr[3].start()
    ring_wo.step(2)
    wo_out(2)
    xr[-2].step(2)
    gu_out(-2)
    xr[2].step(2)
    gu_out(2)
    for dy in (1, 3, 2):
        yf = mod4(y - dy)
        come(resb.at[yf], s_res.at[dy - 1], r_res.at[dy - 1])
        come(gains.at[yf], s_g.at[dy - 1], r_g.at[dy - 1])
    for kk in (-1, 1, 2):
        wo_in(kk)
    for dx, dy in others:
        n = dx * 4 + dy - 1
        come(hb.at[4 * mod4(y - dy) + mod4(x - dx)], s_o.at[n], r_o.at[n])

    attn = None
    for g in range(4):
        heads = [hb[4 * g + 2 * j] + hb[4 * g + 2 * j + 1] for j in range(2)]
        term = jnp.dot(jnp.concatenate(heads, axis=1), wo[g], preferred_element_type=F32)
        term = term.astype(BF).astype(F32)
        attn = term if attn is None else attn + term
    res = jnp.concatenate([resb[g] for g in range(4)], axis=1).astype(F32)
    rows = ALPHA * res + attn
    mean = jnp.sum(rows, axis=1, keepdims=True) * (1.0 / D)
    var = jnp.sum(rows * rows, axis=1, keepdims=True) * (1.0 / D) - mean * mean
    gain = jnp.concatenate([gains[g, 0] for g in range(4)], axis=1)
    hid[y] = ((rows - mean) * lax.rsqrt(var + EPS) * gain).astype(BF)

    ring_h.start()
    ring_gu.step(4)
    xr[4].start()
    xr[-3].step(1)
    xr[3].step(1)
    ring_wdz.step(1)
    wd_out(-1)
    wd_out(1)
    xr[-3].step(2)
    gu_out(-3)
    xr[3].step(2)
    gu_out(3)
    ring_h.step(1)
    xr[4].step(1)
    ring_wdz.step(2)
    wd_out(-2)
    wd_out(2)
    xr[4].step(2)
    gu_out(4)
    for kk in (0, -1, 1, -2, 2, -3, 3, 4):
        gu_in(kk)

    def gate_up(blocks, lo):
        rows = blocks[0] if len(blocks) == 1 else jnp.concatenate(blocks, axis=0)
        n = rows.shape[0]

        def one(j, carry):
            cols = pl.ds(pl.multiple_of(j * QB, QB), QB)
            gate = jnp.dot(rows, wgu[0, :, :, :, :, cols].reshape(D, QB), preferred_element_type=F32)
            up = jnp.dot(rows, wgu[1, :, :, :, :, cols].reshape(D, QB), preferred_element_type=F32)
            mixed[lo : lo + n, cols] = (gate / (1.0 + jnp.exp(-gate)) * up).astype(BF)
            return carry

        lax.fori_loop(0, FC // QB, one, 0)

    def down(slot, count):
        units = mixed[TQ * slot : TQ * (slot + count)]

        def one(j, carry):
            w = wdt[j].reshape(QB, FC)
            got = lax.dot_general(units, w, (((1,), (1,)), ((), ())), preferred_element_type=F32)
            got = got.astype(BF).reshape(count, TQ, QB)
            part[slot : slot + count, :, pl.ds(pl.multiple_of(j * QB, QB), QB)] = got
            return carry

        lax.fori_loop(0, NZ, one, 0)

    dist = (0, -1, 1, 2)

    def send_parts(slots):
        for s in slots:
            for dy in (2, 1, 3):
                yt = mod4(y + dy)
                dst = crec.at[dy - 1, mod4(y + dist[s])]
                go(rcopy(part.at[s, :, cols512(yt)], dst, s_p.at[dy - 1, s], r_p.at[dy - 1, s], ydev(yt)))

    gate_up([hid[y], hid[mod4(y - 1)], hid[mod4(y + 1)]], 0)
    ring_h.step(2)
    ring_wdz.step(3)
    wd_out(-3)
    wd_out(3)
    gate_up([hid[mod4(y + 2)]], 3 * TQ)
    ring_wdz.step(4)
    wd_out(4)
    for kk in (0, -1, 1, -2, 2, -3, 3, 4):
        wd_in(kk)
    down(0, 3)
    send_parts((0, 1, 2))
    down(3, 1)
    send_parts((3,))
    for s in range(4):
        crec[3, mod4(y + dist[s])] = part[s, :, cols512(y)]
    total = crec[3].astype(F32)
    for dy in (1, 3, 2):
        for s in range(4):
            come(crec.at[dy - 1, mod4(y - dy + dist[s])], s_p.at[dy - 1, s], r_p.at[dy - 1, s])
        total = total + crec[dy - 1].astype(F32)
    rows = (ALPHA * hid[:, :, cols512(y)].astype(F32) + HALF * total).reshape(T, 512)
    lane = lax.broadcasted_iota(jnp.int32, (T, 128), 1)
    s1 = jnp.sum(rows, axis=1, keepdims=True)
    s2 = jnp.sum(rows * rows, axis=1, keepdims=True)
    sums = jnp.where(lane == 0, s1, jnp.where(lane == 1, s2, 0.0))
    stat[0] = jnp.transpose(sums)[0:8]
    for dy in (2, 1, 3):
        go(rcopy(stat.at[0], stat.at[dy], s_f.at[dy - 1], r_f.at[dy - 1], ydev(mod4(y + dy))))
    both = stat[0]
    for dy in (1, 3, 2):
        come(stat.at[dy], s_f.at[dy - 1], r_f.at[dy - 1])
        both = both + stat[dy]
    both = jnp.transpose(jnp.concatenate([both, jnp.zeros((120, T), F32)], axis=0))
    mean = both[:, 0:1] * (1.0 / D)
    var = both[:, 1:2] * (1.0 / D) - mean * mean
    out_ref[...] = ((rows - mean) * lax.rsqrt(var + EPS) * gains[y, 1]).astype(BF)
    for cp in log:
        cp.wait_send()


def local(queries, latents, rope_key, w_key, w_value, w_out, resid, gain_mix, w_gate, w_up, w_down, gain_out):
    start = lax.axis_index("sp") * T
    positions = start + jnp.arange(T, dtype=jnp.int32)
    grid_rows = (positions // GRID_W).astype(F32)
    grid_cols = (positions % GRID_W).astype(F32)
    count = ROPE // 4
    inverse = ROTARY_BASE ** (-jnp.arange(count, dtype=F32) / count)
    angles = jnp.concatenate([inverse[:, None] * grid_rows, inverse[:, None] * grid_cols], axis=0)
    cos, sin = jnp.cos(angles), jnp.sin(angles)
    cs = jnp.concatenate([cos, cos], axis=0)
    sn = jnp.concatenate([-sin, sin], axis=0)
    dma = pltpu.SemaphoreType.DMA
    V = pltpu.VMEM

    def pair(*shape):
        return [dma(shape), dma(shape)]

    sems = []
    for shape in (
        (3,), (3,), (3,), (3,),
        (2, 4, 2), (8,), (2, 4), (8, 2, 2), (8,),
        (2, 2), (2, 4), (8,), (2, 2), (3,),
        (15,), (2, 2, 2), (3, 4), (3,),
    ):
        sems += pair(*shape)
    scratch = [
        V((4, 5, TQ, 128), BF),
        V((4, T, 128), BF),
        V((NZ, 2, 5, T, 128), BF),
        V((4, T, 128), BF),
        V((128, NQ), BF),
        V((8 * T, 128), BF),
        V((2, 128, NQ), BF),
        V((2, 8 * T, QB), F32),
        V((2, 8 * T, QB), BF),
        V((128, NQ), F32),
        V((8, NQ), F32),
        V((4, T, 128), BF),
        V((16, TQ, 128), BF),
        V((NY, 256, D), BF),
        V((NY, TQ, 512), BF),
        V((NY, 2, 1, 512), F32),
        V((2, NZ, NX, 2, 32, FC), BF),
        V((NZ, NX, 2, 32, FC), BF),
        V((NY, TQ, D), BF),
        V((T, FC), BF),
        V((NY, TQ, D), BF),
        V((NY, NY, TQ, 512), BF),
        V((NY, 8, T), F32),
    ]
    vm = pl.BlockSpec(memory_space=pltpu.VMEM)
    return pl.pallas_call(
        kernel,
        out_shape=jax.ShapeDtypeStruct((T, 512), BF),
        in_specs=[vm] * 14,
        out_specs=vm,
        scratch_shapes=scratch + sems,
        compiler_params=pltpu.CompilerParams(
            collective_id=0, has_side_effects=True, vmem_limit_bytes=60 * 1024 * 1024
        ),
    )(
        queries, latents, rope_key.T, w_key, w_value, w_out, resid, gain_mix.reshape(1, 512),
        w_gate, w_up, w_down.T, gain_out.reshape(1, 512), cs, sn,
    )


def solution(mesh):
    placed = (
        P("sp", "tp"), P("sp", None), P("sp", None), P(None, "tp"), P(None, "tp"), P("tp", None),
        P("sp", "tp"), P("tp"), P("sp", "tp"), P("sp", "tp"), P("tp", "sp"), P("tp"),
    )
    return jax.shard_map(local, mesh=mesh, in_specs=placed, out_specs=P("sp", "tp"), check_vma=False)
```

time: 101 us -> 94.4 us (0.935)
  local copies, waits for them, and re-layouts: 5.38 us -> 1.62 us
  Pallas kernels: 94.8 us -> 91.2 us
  other arithmetic: 0.19 us -> 1.42 us
    pallas_call x1, Pallas kernels: 94.8 us -> 91.2 us  [local(): pl.pallas_call(kernel, out_shape=jax.ShapeDtypeStruct((T, 512), BF), in_s...]
    unnamed x7 -> x1, local copies, waits for them, and re-layouts: 3.9 us -> 1.62 us
    concatenate x2 -> x0, local copies, waits for them, and re-layouts: 1.48 us -> none  [the longest x1 0.74 us: local(): sn = jnp.concatenate([-sin, sin], axis=1)]
    concatenate x2, other arithmetic: 0.01 us -> 1.24 us  [the longest x1 0.62 us: local(): sn = jnp.concatenate([-sin, sin], axis=0)]
where the time goes in v2:
time: 94.4 us; the launch traced here: 94.3 us
  Pallas kernels  91.2 us (97%)
  local copies, waits for them, and re-layouts  1.62 us (2%)
  other arithmetic  1.42 us (2%)
    pallas_call x1, Pallas kernels, local(): pl.pallas_call(kernel, out_shape=jax.ShapeDtypeStruct((T, 512), BF), in_s...  91.2 us

profile of v2, /device:TPU:1, one launch (start us, length us, event | category | flops | bytes accessed | tf_op | source)
XLA Modules:
  0.0 94.3 jit_solution(5584352280556173206)
XLA Ops:
  0.0 0.1 broadcast_multiply_fusion.1
  0.1 0.1 fusion.5
  0.2 0.6 pad_maximum_fusion.1.sn_ref
  0.8 0.6 pad_maximum_fusion.cs_ref
  1.4 91.2 %shard_map.118 = bf16[192,512]{1,0:T(8,128)(2,1)} custom-call(bf16[192,384]{1,0:T(8,128)(2,1)} %q_ref.1, bf16[192,512]{1,0:T(8,128)(2,1)} %lat_ref.1, bf16[32,192]{1,0:T(8,128)(2,1)} %bitcast.5, bf16[512,256]{1,0:T(8,128)(2,1)} %wk_ref.1, bf16[512,256]{1,0:T(8,128)(2,1)} %wv_ref.1, bf16[256,2048]{1,0:T(8,128)(2,1)} %wo_ref.1, bf16[192,512]{1,0:T(8,128)(2,1)} %res_ref.1, ...), custom_call_target="tpu_custom_call" | custom-call | tf_op jit(solution)/shard_map/pallas_call | solution.py:565
  92.7 1.6 %copy.14 = bf16[192,512]{1,0:T(8,128)(2,1)} copy(bf16[192,512]{1,0:T(8,128)(2,1)} %shard_map.118) | data formatting | bytes 393216
  (2 shorter events, 0.0 us)

commit v3 on v2

--- a/solution.py
+++ b/solution.py
@@ -27,9 +27,13 @@
 
 
 class Ring:
-    def __init__(self, n, pos, dev, blk, half, sems, log, pieces=False):
-        self.n, self.pos, self.dev, self.pieces = n, pos, dev, pieces
+    WHOLE = ((0, None), (1, None))
+    HALVES = ((0, 0), (1, 1))
+
+    def __init__(self, n, pos, dev, blk, half, sems, log, travel=WHOLE, last=HALVES):
+        self.n, self.pos, self.dev, self.travel, self.last = n, pos, dev, travel, last
         self.blk, self.half, self.sems, self.log = blk, half, sems, log
+        self.pieces = travel is not self.WHOLE
 
     def at(self, k):
         return lax.rem(self.pos + (k + 2 * self.n), self.n)
@@ -48,11 +52,7 @@
         )
 
     def parts(self, t):
-        if t == self.n // 2 - 1:
-            return ((0, 0), (1, 1))
-        if self.pieces:
-            return ((0, 0), (1, 1), (0, 1), (1, 0))
-        return ((0, None), (1, None))
+        return self.last if t == self.n // 2 - 1 else self.travel
 
     def send(self, p, d, t, h):
         cp = self.copy(p, d, t, h)
@@ -170,8 +170,10 @@
     ring_kv = Ring(
         NZ, z, zdev,
         lambda p: kvr.at[p, c],
-        lambda p, h: kvr.at[p, c, :, pl.ds(96 * h, 96), :],
-        pairs(s_zkv, r_zkv), log, pieces=True,
+        lambda p, h: kvr.at[p, c, :, rows48(mod4(x - h)), :],
+        pairs(s_zkv, r_zkv), log,
+        travel=tuple((d, h) for h in (0, 1, 3, 2) for d in (0, 1)),
+        last=((0, 0), (1, 3), (0, 1), (1, 2)),
     )
     ring_gu = Ring(
         NZ, z, zdev,
@@ -201,7 +203,8 @@
         NY, y, ydev,
         lambda p: hid.at[p],
         lambda p, h: hid.at[p, :, pl.ds(1024 * h, 1024)],
-        pairs(s_yh, r_yh), log, pieces=True,
+        pairs(s_yh, r_yh), log,
+        travel=((0, 0), (1, 1), (0, 1), (1, 0)),
     )
 
     def gu_ring(k):
@@ -240,13 +243,16 @@
         ref = wo.at[ring_wo.at(k), pl.ds(pl.multiple_of(128 - 128 * c, 128), 128), :]
         come(ref, s_dwo.at[k % NY - 1], r_dwo.at[k % NY - 1])
 
+    kvr[z, c, :, rows48(x), :] = kvsend[x]
+
     pl.semaphore_wait(barrier, len(peers))
 
-    ring_gu.start()
+    for d in (0, 1):
+        ring_kv.send(z, d, 0, 0)
     for dx in (1, 3, 2):
         xt = mod4(x + dx)
         go(rcopy(kvsend.at[xt], kvr.at[z, c, :, rows48(x), :], s_kvx.at[dx - 1], r_kvx.at[dx - 1], xdev(xt)))
-    kvr[z, c, :, rows48(x), :] = kvsend[x]
+    ring_gu.start()
     cs, sn = table[:, :ROPE], table[:, ROPE : 2 * ROPE]
     q = q_ref[...].astype(F32)
     for h in range(4):
@@ -268,13 +274,11 @@
     resb[y] = res_ref[rows48(y), :]
     ring_wo.start()
 
-    ring_gu.step(1)
     for dx in (1, 3, 2):
         come(kvr.at[z, c, :, rows48(mod4(x - dx)), :], s_kvx.at[dx - 1], r_kvx.at[dx - 1])
-    ring_kv.start()
+        for d in (0, 1):
+            ring_kv.send(z, d, 0, dx)
     kv_out(0)
-    xr[-1].start()
-    xr[1].start()
 
     kvt[...] = jnp.ones_like(kvt)
     obuf[...] = jnp.zeros_like(obuf)
@@ -322,13 +326,16 @@
                     acc = got if acc is None else acc + got
             obuf[:, qs] = obuf[:, qs] * factor + acc
 
+    ring_gu.take(1)
+    xr[-1].start()
+    xr[1].start()
     kv_in(0)
     attend(z)
     ring_kv.step(1)
     kv_out(-1)
     kv_out(1)
+    ring_wd.step(1)
     xr[0].step(1)
-    ring_wd.step(1)
     kv_in(-1)
     attend(zk(-1))
     kv_in(1)
@@ -336,15 +343,15 @@
     ring_kv.step(2)
     kv_out(-2)
     kv_out(2)
+    ring_wd.step(2)
+    wd_out(0)
     xr[0].step(2)
     gu_out(0)
-    ring_wd.step(2)
-    wd_out(0)
     xr[-1].step(1)
     xr[1].step(1)
-    ring_gu.take(2)
-    xr[-2].start()
-    xr[2].start()
+    ring_wo.step(1)
+    wo_out(-1)
+    wo_out(1)
     kv_in(-2)
     attend(zk(-2))
     kv_in(2)
@@ -352,25 +359,28 @@
     ring_kv.step(3)
     kv_out(-3)
     kv_out(3)
-    ring_gu.pass_on(2)
-    ring_wdz.start()
+    ring_gu.pass_on(1)
     xr[-1].step(2)
     gu_out(-1)
     xr[1].step(2)
     gu_out(1)
-    ring_wo.step(1)
-    wo_out(-1)
-    wo_out(1)
     kv_in(-3)
     attend(zk(-3))
     ring_kv.step(4)
     kv_out(4)
-    xr[-2].step(1)
-    xr[2].step(1)
+    ring_wo.step(2)
+    wo_out(2)
     kv_in(3)
     attend(zk(3))
+    ring_gu.step(2)
+    xr[-2].start()
+    xr[2].start()
+    ring_wdz.start()
     kv_in(4)
     attend(zk(4))
+    ring_gu.step(3)
+    xr[-3].start()
+    xr[3].start()
 
     par = lax.rem(x, 2).astype(F32)
     on = obuf[HD:128] / obuf[0:1]
@@ -382,15 +392,11 @@
         n = dx * 4 + dy - 1
         go(rcopy(osend.at[xt, rows48(yt), :], hb.at[4 * y + x], s_o.at[n], r_o.at[n], dev(z, xt, c, yt)))
     hb[4 * y + x] = osend[x, rows48(y), :]
-    ring_gu.step(3)
-    xr[-3].start()
-    xr[3].start()
-    ring_wo.step(2)
-    wo_out(2)
-    xr[-2].step(2)
-    gu_out(-2)
-    xr[2].step(2)
-    gu_out(2)
+    xr[-2].step(1)
+    xr[2].step(1)
+    ring_wdz.step(1)
+    wd_out(-1)
+    wd_out(1)
     for dy in (1, 3, 2):
         yf = mod4(y - dy)
         come(resb.at[yf], s_res.at[dy - 1], r_res.at[dy - 1])
@@ -417,20 +423,24 @@
     ring_h.start()
     ring_gu.step(4)
     xr[4].start()
+    xr[-2].step(2)
+    gu_out(-2)
+    xr[2].step(2)
+    gu_out(2)
     xr[-3].step(1)
     xr[3].step(1)
-    ring_wdz.step(1)
-    wd_out(-1)
-    wd_out(1)
+    ring_wdz.step(2)
+    wd_out(-2)
+    wd_out(2)
     xr[-3].step(2)
     gu_out(-3)
     xr[3].step(2)
     gu_out(3)
     ring_h.step(1)
     xr[4].step(1)
-    ring_wdz.step(2)
-    wd_out(-2)
-    wd_out(2)
+    ring_wdz.step(3)
+    wd_out(-3)
+    wd_out(3)
     xr[4].step(2)
     gu_out(4)
     for kk in (0, -1, 1, -2, 2, -3, 3, 4):
@@ -472,12 +482,9 @@
 
     gate_up([hid[y], hid[mod4(y - 1)], hid[mod4(y + 1)]], 0)
     ring_h.step(2)
-    ring_wdz.step(3)
-    wd_out(-3)
-    wd_out(3)
-    gate_up([hid[mod4(y + 2)]], 3 * TQ)
     ring_wdz.step(4)
     wd_out(4)
+    gate_up([hid[mod4(y + 2)]], 3 * TQ)
     for kk in (0, -1, 1, -2, 2, -3, 3, 4):
         wd_in(kk)
     down(0, 3)
@@ -531,7 +538,7 @@
     sems = []
     for shape in (
         (3,), (3,), (3,), (3,),
-        (2, 4, 2), (8,), (2, 4), (8, 2, 2), (8,),
+        (2, 4, 4), (8,), (2, 4), (8, 2, 2), (8,),
         (2, 2), (2, 4), (8,), (2, 2), (3,),
         (15,), (2, 2, 2), (3, 4), (3,),
     ):

time: 94.4 us -> 95.4 us (1.011)
  Pallas kernels: 91.2 us -> 92.3 us
    pallas_call x1, Pallas kernels: 91.2 us -> 92.3 us  [local(): pl.pallas_call(kernel, out_shape=jax.ShapeDtypeStruct((T, 512), BF), in_s...]
where the time goes in v3:
time: 95.4 us; the launch traced here: 95.3 us
  Pallas kernels  92.3 us (97%)
  local copies, waits for them, and re-layouts  1.62 us (2%)
  other arithmetic  1.42 us (1%)
    pallas_call x1, Pallas kernels, local(): pl.pallas_call(kernel, out_shape=jax.ShapeDtypeStruct((T, 512), BF), in_s...  92.3 us

profile of v3, /device:TPU:1, one launch (start us, length us, event | category | flops | bytes accessed | tf_op | source)
XLA Modules:
  0.0 95.3 jit_solution(17913845662340323088)
XLA Ops:
  0.0 0.1 broadcast_multiply_fusion.1
  0.1 0.1 fusion.5
  0.2 0.6 pad_maximum_fusion.1.sn_ref
  0.8 0.6 pad_maximum_fusion.cs_ref
  1.4 92.3 %shard_map.118 = bf16[192,512]{1,0:T(8,128)(2,1)} custom-call(bf16[192,384]{1,0:T(8,128)(2,1)} %q_ref.1, bf16[192,512]{1,0:T(8,128)(2,1)} %lat_ref.1, bf16[32,192]{1,0:T(8,128)(2,1)} %bitcast.5, bf16[512,256]{1,0:T(8,128)(2,1)} %wk_ref.1, bf16[512,256]{1,0:T(8,128)(2,1)} %wv_ref.1, bf16[256,2048]{1,0:T(8,128)(2,1)} %wo_ref.1, bf16[192,512]{1,0:T(8,128)(2,1)} %res_ref.1, ...), custom_call_target="tpu_custom_call" | custom-call | tf_op jit(solution)/shard_map/pallas_call | solution.py:572
  93.7 1.6 %copy.14 = bf16[192,512]{1,0:T(8,128)(2,1)} copy(bf16[192,512]{1,0:T(8,128)(2,1)} %shard_map.118) | data formatting | bytes 393216
  (2 shorter events, 0.0 us)

commit v4 on v3

--- a/solution.py
+++ b/solution.py
@@ -88,10 +88,9 @@
     q_ref, lat_ref, rk_ref, wk_ref, wv_ref, wo_ref, res_ref, gm_ref, wg_ref, wu_ref, wd_ref, go_ref, cs_ref, sn_ref,
     out_ref,
     kvsend, qsend, kvr, qin, qt, kp, kvt, sbuf, pbuf, obuf, mbuf, osend, hb, wo, resb, gains,
-    wgu, wdt, hid, mixed, part, crec, stat,
+    w3, hid, mixed, part, crec, acc, stat,
     s_kvx, r_kvx, s_qx, r_qx, s_res, r_res, s_g, r_g,
-    s_zkv, r_zkv, s_dkv, r_dkv, s_zgu, r_zgu, s_xgu, r_xgu, s_dgu, r_dgu,
-    s_xwd, r_xwd, s_zwd, r_zwd, s_dwd, r_dwd, s_ywo, r_ywo, s_dwo, r_dwo,
+    s_zkv, r_zkv, s_dkv, r_dkv, s_zw, r_zw, s_xw, r_xw, s_dw, r_dw, s_ywo, r_ywo, s_dwo, r_dwo,
     s_o, r_o, s_yh, r_yh, s_p, r_p, s_f, r_f,
 ):
     sp = lax.axis_index("sp")
@@ -139,9 +138,9 @@
     for peer in peers:
         pl.semaphore_signal(barrier, inc=1, device_id=peer, device_id_type=MESH)
 
-    wgu[0, z, x, c] = wg_ref[...]
-    wgu[1, z, x, c] = wu_ref[...]
-    wdt[z, x, c] = wd_ref[...]
+    w3[0, z, x, c] = wg_ref[...]
+    w3[1, z, x, c] = wu_ref[...]
+    w3[2, z, x, c] = wd_ref[...]
     wo[y] = wo_ref[...]
     gains[y, 0] = gm_ref[...]
     gains[y, 1] = go_ref[...]
@@ -175,23 +174,11 @@
         travel=tuple((d, h) for h in (0, 1, 3, 2) for d in (0, 1)),
         last=((0, 0), (1, 3), (0, 1), (1, 2)),
     )
-    ring_gu = Ring(
+    ring_w = Ring(
         NZ, z, zdev,
-        lambda p: wgu.at[:, p, x, c],
-        lambda p, h: wgu.at[:, p, x, c, pl.ds(16 * h, 16), :],
-        pairs(s_zgu, r_zgu), log,
-    )
-    ring_wd = Ring(
-        NX, x, xdev,
-        lambda p: wdt.at[z, p, c],
-        lambda p, h: wdt.at[z, p, c, pl.ds(16 * h, 16), :],
-        pairs(s_xwd, r_xwd), log,
-    )
-    ring_wdz = Ring(
-        NZ, z, zdev,
-        lambda p: wdt.at[p, :, c],
-        lambda p, h: wdt.at[p, pl.ds(2 * h, 2), c],
-        pairs(s_zwd, r_zwd), log,
+        lambda p: w3.at[:, p, x, c],
+        lambda p, h: w3.at[:, p, x, c, pl.ds(16 * h, 16), :],
+        pairs(s_zw, r_zw), log,
     )
     ring_wo = Ring(
         NY, y, ydev,
@@ -207,16 +194,16 @@
         travel=((0, 0), (1, 1), (0, 1), (1, 0)),
     )
 
-    def gu_ring(k):
+    def x_ring(k):
         p = zk(k)
         return Ring(
             NX, x, xdev,
-            lambda q: wgu.at[:, p, q, c],
-            lambda q, h: wgu.at[:, p, q, c, pl.ds(16 * h, 16), :],
-            [(s_xgu.at[k % NZ, d], r_xgu.at[k % NZ, d]) for d in (0, 1)], log,
+            lambda q: w3.at[:, p, q, c],
+            lambda q, h: w3.at[:, p, q, c, pl.ds(16 * h, 16), :],
+            [(s_xw.at[k % NZ, d], r_xw.at[k % NZ, d]) for d in (0, 1)], log,
         )
 
-    xr = {k: gu_ring(k) for k in (0, -1, 1, -2, 2, -3, 3, 4)}
+    xr = {k: x_ring(k) for k in (0, -1, 1, -2, 2, -3, 3, 4)}
 
     def kv_out(k):
         to_partner(kvr.at[zk(k), c], s_dkv.at[k % NZ], r_dkv.at[k % NZ])
@@ -224,17 +211,11 @@
     def kv_in(k):
         come(kvr.at[zk(k), 1 - c], s_dkv.at[k % NZ], r_dkv.at[k % NZ])
 
-    def gu_out(k):
-        to_partner(wgu.at[:, zk(k), :, c], s_dgu.at[k % NZ], r_dgu.at[k % NZ])
-
-    def gu_in(k):
-        come(wgu.at[:, zk(k), :, 1 - c], s_dgu.at[k % NZ], r_dgu.at[k % NZ])
-
-    def wd_out(k):
-        to_partner(wdt.at[zk(k), :, c], s_dwd.at[k % NZ], r_dwd.at[k % NZ])
-
-    def wd_in(k):
-        come(wdt.at[zk(k), :, 1 - c], s_dwd.at[k % NZ], r_dwd.at[k % NZ])
+    def w_out(k):
+        to_partner(w3.at[:, zk(k), :, c], s_dw.at[k % NZ], r_dw.at[k % NZ])
+
+    def w_in(k):
+        come(w3.at[:, zk(k), :, 1 - c], s_dw.at[k % NZ], r_dw.at[k % NZ])
 
     def wo_out(k):
         to_partner(ring_wo.blk(ring_wo.at(k)), s_dwo.at[k % NY - 1], r_dwo.at[k % NY - 1])
@@ -245,14 +226,6 @@
 
     kvr[z, c, :, rows48(x), :] = kvsend[x]
 
-    pl.semaphore_wait(barrier, len(peers))
-
-    for d in (0, 1):
-        ring_kv.send(z, d, 0, 0)
-    for dx in (1, 3, 2):
-        xt = mod4(x + dx)
-        go(rcopy(kvsend.at[xt], kvr.at[z, c, :, rows48(x), :], s_kvx.at[dx - 1], r_kvx.at[dx - 1], xdev(xt)))
-    ring_gu.start()
     cs, sn = table[:, :ROPE], table[:, ROPE : 2 * ROPE]
     q = q_ref[...].astype(F32)
     for h in range(4):
@@ -260,18 +233,29 @@
         turned = qr * cs + jnp.concatenate([qr[:, ROPE // 2 :], qr[:, : ROPE // 2]], axis=1) * sn
         full = jnp.concatenate([q[:, 96 * h : 96 * h + HD], turned, jnp.zeros((T, 32), F32)], axis=1)
         qsend[h] = full.astype(BF)
+    qin[x] = qsend[x]
+    resb[y] = res_ref[rows48(y), :]
+    kvt[...] = jnp.ones_like(kvt)
+    obuf[...] = jnp.zeros_like(obuf)
+    mbuf[...] = jnp.full_like(mbuf, -1e30)
+
+    pl.semaphore_wait(barrier, len(peers))
+
+    for d in (0, 1):
+        ring_kv.send(z, d, 0, 0)
+    for dx in (1, 3, 2):
+        xt = mod4(x + dx)
+        go(rcopy(kvsend.at[xt], kvr.at[z, c, :, rows48(x), :], s_kvx.at[dx - 1], r_kvx.at[dx - 1], xdev(xt)))
+    ring_w.start()
     for dx in (1, 3, 2):
         xt = mod4(x + dx)
         go(rcopy(qsend.at[xt], qin.at[x], s_qx.at[dx - 1], r_qx.at[dx - 1], xdev(xt)))
-    qin[x] = qsend[x]
     xr[0].start()
-    ring_wd.start()
 
     for dy in (1, 3, 2):
         yt = mod4(y + dy)
         go(rcopy(res_ref.at[rows48(yt), :], resb.at[y], s_res.at[dy - 1], r_res.at[dy - 1], ydev(yt)))
         go(rcopy(gains.at[y], gains.at[y], s_g.at[dy - 1], r_g.at[dy - 1], ydev(yt)))
-    resb[y] = res_ref[rows48(y), :]
     ring_wo.start()
 
     for dx in (1, 3, 2):
@@ -280,9 +264,6 @@
             ring_kv.send(z, d, 0, dx)
     kv_out(0)
 
-    kvt[...] = jnp.ones_like(kvt)
-    obuf[...] = jnp.zeros_like(obuf)
-    mbuf[...] = jnp.full_like(mbuf, -1e30)
     for dx in (1, 3, 2):
         come(qin.at[mod4(x - dx)], s_qx.at[dx - 1], r_qx.at[dx - 1])
     qt[...] = jnp.transpose(qin[...].reshape(NQ, 128))
@@ -326,7 +307,7 @@
                     acc = got if acc is None else acc + got
             obuf[:, qs] = obuf[:, qs] * factor + acc
 
-    ring_gu.take(1)
+    ring_w.take(1)
     xr[-1].start()
     xr[1].start()
     kv_in(0)
@@ -334,7 +315,7 @@
     ring_kv.step(1)
     kv_out(-1)
     kv_out(1)
-    ring_wd.step(1)
+    ring_w.pass_on(1)
     xr[0].step(1)
     kv_in(-1)
     attend(zk(-1))
@@ -343,27 +324,28 @@
     ring_kv.step(2)
     kv_out(-2)
     kv_out(2)
-    ring_wd.step(2)
-    wd_out(0)
     xr[0].step(2)
-    gu_out(0)
+    w_out(0)
     xr[-1].step(1)
     xr[1].step(1)
-    ring_wo.step(1)
-    wo_out(-1)
-    wo_out(1)
     kv_in(-2)
     attend(zk(-2))
     kv_in(2)
     attend(zk(2))
+    ring_w.take(2)
+    xr[-2].start()
+    xr[2].start()
     ring_kv.step(3)
     kv_out(-3)
     kv_out(3)
-    ring_gu.pass_on(1)
+    ring_w.pass_on(2)
     xr[-1].step(2)
-    gu_out(-1)
+    w_out(-1)
     xr[1].step(2)
-    gu_out(1)
+    w_out(1)
+    ring_wo.step(1)
+    wo_out(-1)
+    wo_out(1)
     kv_in(-3)
     attend(zk(-3))
     ring_kv.step(4)
@@ -372,13 +354,11 @@
     wo_out(2)
     kv_in(3)
     attend(zk(3))
-    ring_gu.step(2)
-    xr[-2].start()
-    xr[2].start()
-    ring_wdz.start()
+    xr[-2].step(1)
+    xr[2].step(1)
     kv_in(4)
     attend(zk(4))
-    ring_gu.step(3)
+    ring_w.step(3)
     xr[-3].start()
     xr[3].start()
 
@@ -392,11 +372,12 @@
         n = dx * 4 + dy - 1
         go(rcopy(osend.at[xt, rows48(yt), :], hb.at[4 * y + x], s_o.at[n], r_o.at[n], dev(z, xt, c, yt)))
     hb[4 * y + x] = osend[x, rows48(y), :]
-    xr[-2].step(1)
-    xr[2].step(1)
-    ring_wdz.step(1)
-    wd_out(-1)
-    wd_out(1)
+    xr[-2].step(2)
+    w_out(-2)
+    xr[2].step(2)
+    w_out(2)
+    ring_w.step(4)
+    xr[4].start()
     for dy in (1, 3, 2):
         yf = mod4(y - dy)
         come(resb.at[yf], s_res.at[dy - 1], r_res.at[dy - 1])
@@ -421,30 +402,18 @@
     hid[y] = ((rows - mean) * lax.rsqrt(var + EPS) * gain).astype(BF)
 
     ring_h.start()
-    ring_gu.step(4)
-    xr[4].start()
-    xr[-2].step(2)
-    gu_out(-2)
-    xr[2].step(2)
-    gu_out(2)
     xr[-3].step(1)
     xr[3].step(1)
-    ring_wdz.step(2)
-    wd_out(-2)
-    wd_out(2)
+    xr[4].step(1)
+    ring_h.step(1)
     xr[-3].step(2)
-    gu_out(-3)
+    w_out(-3)
     xr[3].step(2)
-    gu_out(3)
-    ring_h.step(1)
-    xr[4].step(1)
-    ring_wdz.step(3)
-    wd_out(-3)
-    wd_out(3)
+    w_out(3)
     xr[4].step(2)
-    gu_out(4)
+    w_out(4)
     for kk in (0, -1, 1, -2, 2, -3, 3, 4):
-        gu_in(kk)
+        w_in(kk)
 
     def gate_up(blocks, lo):
         rows = blocks[0] if len(blocks) == 1 else jnp.concatenate(blocks, axis=0)
@@ -452,52 +421,45 @@
 
         def one(j, carry):
             cols = pl.ds(pl.multiple_of(j * QB, QB), QB)
-            gate = jnp.dot(rows, wgu[0, :, :, :, :, cols].reshape(D, QB), preferred_element_type=F32)
-            up = jnp.dot(rows, wgu[1, :, :, :, :, cols].reshape(D, QB), preferred_element_type=F32)
+            gate = jnp.dot(rows, w3[0, :, :, :, :, cols].reshape(D, QB), preferred_element_type=F32)
+            up = jnp.dot(rows, w3[1, :, :, :, :, cols].reshape(D, QB), preferred_element_type=F32)
             mixed[lo : lo + n, cols] = (gate / (1.0 + jnp.exp(-gate)) * up).astype(BF)
             return carry
 
         lax.fori_loop(0, FC // QB, one, 0)
 
+    dist = (0, -1, 1, 2)
+
     def down(slot, count):
         units = mixed[TQ * slot : TQ * (slot + count)]
-
-        def one(j, carry):
-            w = wdt[j].reshape(QB, FC)
+        slots = slice(slot, slot + count)
+        for dy in (2, 1, 3, 0):
+            yt = mod4(y + dy)
+            w = w3[2, pl.ds(2 * yt, 2)].reshape(512, FC)
             got = lax.dot_general(units, w, (((1,), (1,)), ((), ())), preferred_element_type=F32)
-            got = got.astype(BF).reshape(count, TQ, QB)
-            part[slot : slot + count, :, pl.ds(pl.multiple_of(j * QB, QB), QB)] = got
-            return carry
-
-        lax.fori_loop(0, NZ, one, 0)
-
-    dist = (0, -1, 1, 2)
-
-    def send_parts(slots):
-        for s in slots:
-            for dy in (2, 1, 3):
-                yt = mod4(y + dy)
-                dst = crec.at[dy - 1, mod4(y + dist[s])]
-                go(rcopy(part.at[s, :, cols512(yt)], dst, s_p.at[dy - 1, s], r_p.at[dy - 1, s], ydev(yt)))
+            got = got.astype(BF).reshape(count, TQ, 512)
+            if dy:
+                n = min(slot, 1)
+                part[dy - 1, slots] = got
+                src = part.at[dy - 1, pl.ds(slot, count)]
+                dst = crec.at[dy - 1, pl.ds(slot, count)]
+                go(rcopy(src, dst, s_p.at[dy - 1, n], r_p.at[dy - 1, n], ydev(yt)))
+            else:
+                for s in range(count):
+                    acc[mod4(y + dist[slot + s])] = got[s].astype(F32)
 
     gate_up([hid[y], hid[mod4(y - 1)], hid[mod4(y + 1)]], 0)
+    down(0, 3)
     ring_h.step(2)
-    ring_wdz.step(4)
-    wd_out(4)
     gate_up([hid[mod4(y + 2)]], 3 * TQ)
-    for kk in (0, -1, 1, -2, 2, -3, 3, 4):
-        wd_in(kk)
-    down(0, 3)
-    send_parts((0, 1, 2))
     down(3, 1)
-    send_parts((3,))
-    for s in range(4):
-        crec[3, mod4(y + dist[s])] = part[s, :, cols512(y)]
-    total = crec[3].astype(F32)
-    for dy in (1, 3, 2):
-        for s in range(4):
-            come(crec.at[dy - 1, mod4(y - dy + dist[s])], s_p.at[dy - 1, s], r_p.at[dy - 1, s])
-        total = total + crec[dy - 1].astype(F32)
+    for n, slots in ((0, (0, 1, 2)), (1, (3,))):
+        for dy in (1, 3, 2):
+            come(crec.at[dy - 1, pl.ds(slots[0], len(slots))], s_p.at[dy - 1, n], r_p.at[dy - 1, n])
+            for s in slots:
+                b = mod4(y - dy + dist[s])
+                acc[b] = acc[b] + crec[dy - 1, s].astype(F32)
+    total = acc[...]
     rows = (ALPHA * hid[:, :, cols512(y)].astype(F32) + HALF * total).reshape(T, 512)
     lane = lax.broadcasted_iota(jnp.int32, (T, 128), 1)
     s1 = jnp.sum(rows, axis=1, keepdims=True)
@@ -539,8 +501,8 @@
     for shape in (
         (3,), (3,), (3,), (3,),
         (2, 4, 4), (8,), (2, 4), (8, 2, 2), (8,),
-        (2, 2), (2, 4), (8,), (2, 2), (3,),
-        (15,), (2, 2, 2), (3, 4), (3,),
+        (2, 2), (3,),
+        (15,), (2, 2, 2), (3, 2), (3,),
     ):
         sems += pair(*shape)
     scratch = [
@@ -560,12 +522,12 @@
         V((NY, 256, D), BF),
         V((NY, TQ, 512), BF),
         V((NY, 2, 1, 512), F32),
-        V((2, NZ, NX, 2, 32, FC), BF),
-        V((NZ, NX, 2, 32, FC), BF),
+        V((3, NZ, NX, 2, 32, FC), BF),
         V((NY, TQ, D), BF),
         V((T, FC), BF),
-        V((NY, TQ, D), BF),
-        V((NY, NY, TQ, 512), BF),
+        V((3, NY, TQ, 512), BF),
+        V((3, NY, TQ, 512), BF),
+        V((NY, TQ, 512), F32),
         V((NY, 8, T), F32),
     ]
     vm = pl.BlockSpec(memory_space=pltpu.VMEM)

time: 95.4 us -> 91.3 us (0.957)
  Pallas kernels: 92.3 us -> 88.2 us
    pallas_call x1, Pallas kernels: 92.3 us -> 88.2 us  [local(): pl.pallas_call(kernel, out_shape=jax.ShapeDtypeStruct((T, 512), BF), in_s...]
where the time goes in v4:
time: 91.3 us; the launch traced here: 91.2 us
  Pallas kernels  88.2 us (97%)
  local copies, waits for them, and re-layouts  1.62 us (2%)
  other arithmetic  1.42 us (2%)
    pallas_call x1, Pallas kernels, local(): pl.pallas_call(kernel, out_shape=jax.ShapeDtypeStruct((T, 512), BF), in_s...  88.2 us

profile of v4, /device:TPU:1, one launch (start us, length us, event | category | flops | bytes accessed | tf_op | source)
XLA Modules:
  0.0 91.2 jit_solution(8763363838754661386)
XLA Ops:
  0.0 0.1 broadcast_multiply_fusion.1
  0.1 0.1 fusion.5
  0.2 0.6 pad_maximum_fusion.1.sn_ref
  0.8 0.6 pad_maximum_fusion.cs_ref
  1.4 88.2 %shard_map.118 = bf16[192,512]{1,0:T(8,128)(2,1)} custom-call(bf16[192,384]{1,0:T(8,128)(2,1)} %q_ref.1, bf16[192,512]{1,0:T(8,128)(2,1)} %lat_ref.1, bf16[32,192]{1,0:T(8,128)(2,1)} %bitcast.5, bf16[512,256]{1,0:T(8,128)(2,1)} %wk_ref.1, bf16[512,256]{1,0:T(8,128)(2,1)} %wv_ref.1, bf16[256,2048]{1,0:T(8,128)(2,1)} %wo_ref.1, bf16[192,512]{1,0:T(8,128)(2,1)} %res_ref.1, ...), custom_call_target="tpu_custom_call" | custom-call | tf_op jit(solution)/shard_map/pallas_call | solution.py:534
  89.6 1.6 %copy.14 = bf16[192,512]{1,0:T(8,128)(2,1)} copy(bf16[192,512]{1,0:T(8,128)(2,1)} %shard_map.118) | data formatting | bytes 393216
  (2 shorter events, 0.0 us)

commit v5 on v4

--- a/solution.py
+++ b/solution.py
@@ -263,6 +263,7 @@
         for d in (0, 1):
             ring_kv.send(z, d, 0, dx)
     kv_out(0)
+    ring_w.step(1)
 
     for dx in (1, 3, 2):
         come(qin.at[mod4(x - dx)], s_qx.at[dx - 1], r_qx.at[dx - 1])
@@ -307,7 +308,6 @@
                     acc = got if acc is None else acc + got
             obuf[:, qs] = obuf[:, qs] * factor + acc
 
-    ring_w.take(1)
     xr[-1].start()
     xr[1].start()
     kv_in(0)
@@ -315,15 +315,18 @@
     ring_kv.step(1)
     kv_out(-1)
     kv_out(1)
-    ring_w.pass_on(1)
     xr[0].step(1)
     kv_in(-1)
     attend(zk(-1))
+    ring_w.take(2)
+    xr[-2].start()
+    xr[2].start()
     kv_in(1)
     attend(zk(1))
     ring_kv.step(2)
     kv_out(-2)
     kv_out(2)
+    ring_w.pass_on(2)
     xr[0].step(2)
     w_out(0)
     xr[-1].step(1)
@@ -332,17 +335,15 @@
     attend(zk(-2))
     kv_in(2)
     attend(zk(2))
-    ring_w.take(2)
-    xr[-2].start()
-    xr[2].start()
     ring_kv.step(3)
     kv_out(-3)
     kv_out(3)
-    ring_w.pass_on(2)
     xr[-1].step(2)
     w_out(-1)
     xr[1].step(2)
     w_out(1)
+    xr[-2].step(1)
+    xr[2].step(1)
     ring_wo.step(1)
     wo_out(-1)
     wo_out(1)
@@ -350,17 +351,21 @@
     attend(zk(-3))
     ring_kv.step(4)
     kv_out(4)
+    ring_w.step(3)
+    xr[-3].start()
+    xr[3].start()
     ring_wo.step(2)
     wo_out(2)
     kv_in(3)
     attend(zk(3))
-    xr[-2].step(1)
-    xr[2].step(1)
+    xr[-2].step(2)
+    w_out(-2)
+    xr[2].step(2)
+    w_out(2)
     kv_in(4)
     attend(zk(4))
-    ring_w.step(3)
-    xr[-3].start()
-    xr[3].start()
+    ring_w.take(4)
+    xr[4].start()
 
     par = lax.rem(x, 2).astype(F32)
     on = obuf[HD:128] / obuf[0:1]
@@ -372,12 +377,6 @@
         n = dx * 4 + dy - 1
         go(rcopy(osend.at[xt, rows48(yt), :], hb.at[4 * y + x], s_o.at[n], r_o.at[n], dev(z, xt, c, yt)))
     hb[4 * y + x] = osend[x, rows48(y), :]
-    xr[-2].step(2)
-    w_out(-2)
-    xr[2].step(2)
-    w_out(2)
-    ring_w.step(4)
-    xr[4].start()
     for dy in (1, 3, 2):
         yf = mod4(y - dy)
         come(resb.at[yf], s_res.at[dy - 1], r_res.at[dy - 1])
@@ -405,11 +404,11 @@
     xr[-3].step(1)
     xr[3].step(1)
     xr[4].step(1)
-    ring_h.step(1)
     xr[-3].step(2)
     w_out(-3)
     xr[3].step(2)
     w_out(3)
+    ring_h.step(1)
     xr[4].step(2)
     w_out(4)
     for kk in (0, -1, 1, -2, 2, -3, 3, 4):

time: 91.3 us -> 89.9 us (0.985)
  Pallas kernels: 88.2 us -> 86.7 us
    pallas_call x1, Pallas kernels: 88.2 us -> 86.7 us  [local(): pl.pallas_call(kernel, out_shape=jax.ShapeDtypeStruct((T, 512), BF), in_s...]
where the time goes in v5:
time: 89.9 us; the launch traced here: 89.8 us
  Pallas kernels  86.7 us (96%)
  local copies, waits for them, and re-layouts  1.62 us (2%)
  other arithmetic  1.42 us (2%)
    pallas_call x1, Pallas kernels, local(): pl.pallas_call(kernel, out_shape=jax.ShapeDtypeStruct((T, 512), BF), in_s...  86.7 us

profile of v5, /device:TPU:1, one launch (start us, length us, event | category | flops | bytes accessed | tf_op | source)
XLA Modules:
  0.0 89.8 jit_solution(550984083159784510)
XLA Ops:
  0.0 0.1 broadcast_multiply_fusion.1
  0.1 0.1 fusion.5
  0.2 0.6 pad_maximum_fusion.1.sn_ref
  0.8 0.6 pad_maximum_fusion.cs_ref
  1.4 86.7 %shard_map.118 = bf16[192,512]{1,0:T(8,128)(2,1)} custom-call(bf16[192,384]{1,0:T(8,128)(2,1)} %q_ref.1, bf16[192,512]{1,0:T(8,128)(2,1)} %lat_ref.1, bf16[32,192]{1,0:T(8,128)(2,1)} %bitcast.5, bf16[512,256]{1,0:T(8,128)(2,1)} %wk_ref.1, bf16[512,256]{1,0:T(8,128)(2,1)} %wv_ref.1, bf16[256,2048]{1,0:T(8,128)(2,1)} %wo_ref.1, bf16[192,512]{1,0:T(8,128)(2,1)} %res_ref.1, ...), custom_call_target="tpu_custom_call" | custom-call | tf_op jit(solution)/shard_map/pallas_call | solution.py:533
  88.1 1.6 %copy.14 = bf16[192,512]{1,0:T(8,128)(2,1)} copy(bf16[192,512]{1,0:T(8,128)(2,1)} %shard_map.118) | data formatting | bytes 393216
  (2 shorter events, 0.0 us)

commit v6 on v5

--- a/solution.py
+++ b/solution.py
@@ -88,7 +88,7 @@
     q_ref, lat_ref, rk_ref, wk_ref, wv_ref, wo_ref, res_ref, gm_ref, wg_ref, wu_ref, wd_ref, go_ref, cs_ref, sn_ref,
     out_ref,
     kvsend, qsend, kvr, qin, qt, kp, kvt, sbuf, pbuf, obuf, mbuf, osend, hb, wo, resb, gains,
-    w3, hid, mixed, part, crec, acc, stat,
+    w3, hid, gacc, mixed, part, crec, acc, stat,
     s_kvx, r_kvx, s_qx, r_qx, s_res, r_res, s_g, r_g,
     s_zkv, r_zkv, s_dkv, r_dkv, s_zw, r_zw, s_xw, r_xw, s_dw, r_dw, s_ywo, r_ywo, s_dwo, r_dwo,
     s_o, r_o, s_yh, r_yh, s_p, r_p, s_f, r_f,
@@ -203,7 +203,12 @@
             [(s_xw.at[k % NZ, d], r_xw.at[k % NZ, d]) for d in (0, 1)], log,
         )
 
-    xr = {k: x_ring(k) for k in (0, -1, 1, -2, 2, -3, 3, 4)}
+    xr = {k: x_ring(k) for k in (0, -1, 1, -2, 2, -3, 3)}
+
+    def last_x(dx, slot):
+        ref = w3.at[:, zk(4), slot, c]
+        at = (4, (dx - 1) // 2, (dx - 1) % 2)
+        return rcopy(ref, ref, s_xw.at[at], r_xw.at[at], xdev(mod4(x + dx)))
 
     def kv_out(k):
         to_partner(kvr.at[zk(k), c], s_dkv.at[k % NZ], r_dkv.at[k % NZ])
@@ -365,7 +370,8 @@
     kv_in(4)
     attend(zk(4))
     ring_w.take(4)
-    xr[4].start()
+    for dx in (2, 1, 3):
+        go(last_x(dx, x))
 
     par = lax.rem(x, 2).astype(F32)
     on = obuf[HD:128] / obuf[0:1]
@@ -386,6 +392,8 @@
     for dx, dy in others:
         n = dx * 4 + dy - 1
         come(hb.at[4 * mod4(y - dy) + mod4(x - dx)], s_o.at[n], r_o.at[n])
+    xr[-3].step(1)
+    xr[3].step(1)
 
     attn = None
     for g in range(4):
@@ -401,18 +409,29 @@
     hid[y] = ((rows - mean) * lax.rsqrt(var + EPS) * gain).astype(BF)
 
     ring_h.start()
-    xr[-3].step(1)
-    xr[3].step(1)
-    xr[4].step(1)
     xr[-3].step(2)
     w_out(-3)
     xr[3].step(2)
     w_out(3)
     ring_h.step(1)
-    xr[4].step(2)
+
+    def gate_up_block(k, first):
+        w_in(k)
+        cols = pl.ds(pl.multiple_of(256 * zk(k), 256), 256)
+        some = jnp.concatenate([hid[b, :, cols] for b in (y, mod4(y - 1), mod4(y + 1))], axis=0)
+        for n in (0, 1):
+            term = jnp.dot(some, w3[n, zk(k)].reshape(256, FC), preferred_element_type=F32)
+            gacc[n] = term if first else gacc[n] + term
+
+    for kk in (0, -1, 1, -2, 2):
+        gate_up_block(kk, kk == 0)
+    for dx in (1, 3, 2):
+        last_x(dx, mod4(x - dx)).wait_recv()
     w_out(4)
-    for kk in (0, -1, 1, -2, 2, -3, 3, 4):
-        w_in(kk)
+    for kk in (-3, 3, 4):
+        gate_up_block(kk, False)
+    gate = gacc[0]
+    mixed[0 : 3 * TQ] = (gate / (1.0 + jnp.exp(-gate)) * gacc[1]).astype(BF)
 
     def gate_up(blocks, lo):
         rows = blocks[0] if len(blocks) == 1 else jnp.concatenate(blocks, axis=0)
@@ -447,7 +466,6 @@
                 for s in range(count):
                     acc[mod4(y + dist[slot + s])] = got[s].astype(F32)
 
-    gate_up([hid[y], hid[mod4(y - 1)], hid[mod4(y + 1)]], 0)
     down(0, 3)
     ring_h.step(2)
     gate_up([hid[mod4(y + 2)]], 3 * TQ)
@@ -523,6 +541,7 @@
         V((NY, 2, 1, 512), F32),
         V((3, NZ, NX, 2, 32, FC), BF),
         V((NY, TQ, D), BF),
+        V((2, 3 * TQ, FC), F32),
         V((T, FC), BF),
         V((3, NY, TQ, 512), BF),
         V((3, NY, TQ, 512), BF),

time: 89.9 us -> 92.3 us (1.027)
  Pallas kernels: 86.7 us -> 89.1 us
    pallas_call x1, Pallas kernels: 86.7 us -> 89.1 us  [local(): pl.pallas_call(kernel, out_shape=jax.ShapeDtypeStruct((T, 512), BF), in_s...]
where the time goes in v6:
time: 92.3 us; the launch traced here: 92.1 us
  Pallas kernels  89.1 us (97%)
  local copies, waits for them, and re-layouts  1.62 us (2%)
  other arithmetic  1.42 us (2%)
    pallas_call x1, Pallas kernels, local(): pl.pallas_call(kernel, out_shape=jax.ShapeDtypeStruct((T, 512), BF), in_s...  89.1 us

profile of v6, /device:TPU:1, one launch (start us, length us, event | category | flops | bytes accessed | tf_op | source)
XLA Modules:
  0.0 92.1 jit_solution(14990379000686995432)
XLA Ops:
  0.0 0.1 broadcast_multiply_fusion.1
  0.1 0.1 fusion.5
  0.2 0.6 pad_maximum_fusion.1.sn_ref
  0.8 0.6 pad_maximum_fusion.cs_ref
  1.4 89.1 %shard_map.118 = bf16[192,512]{1,0:T(8,128)(2,1)} custom-call(bf16[192,384]{1,0:T(8,128)(2,1)} %q_ref.1, bf16[192,512]{1,0:T(8,128)(2,1)} %lat_ref.1, bf16[32,192]{1,0:T(8,128)(2,1)} %bitcast.5, bf16[512,256]{1,0:T(8,128)(2,1)} %wk_ref.1, bf16[512,256]{1,0:T(8,128)(2,1)} %wv_ref.1, bf16[256,2048]{1,0:T(8,128)(2,1)} %wo_ref.1, bf16[192,512]{1,0:T(8,128)(2,1)} %res_ref.1, ...), custom_call_target="tpu_custom_call" | custom-call | tf_op jit(solution)/shard_map/pallas_call | solution.py:552
  90.5 1.6 %copy.14 = bf16[192,512]{1,0:T(8,128)(2,1)} copy(bf16[192,512]{1,0:T(8,128)(2,1)} %shard_map.118) | data formatting | bytes 393216
  (2 shorter events, 0.0 us)

commit v7 on v5

--- a/solution.py
+++ b/solution.py
@@ -386,6 +386,8 @@
     for dx, dy in others:
         n = dx * 4 + dy - 1
         come(hb.at[4 * mod4(y - dy) + mod4(x - dx)], s_o.at[n], r_o.at[n])
+    xr[-3].step(1)
+    xr[3].step(1)
 
     attn = None
     for g in range(4):
@@ -401,8 +403,6 @@
     hid[y] = ((rows - mean) * lax.rsqrt(var + EPS) * gain).astype(BF)
 
     ring_h.start()
-    xr[-3].step(1)
-    xr[3].step(1)
     xr[4].step(1)
     xr[-3].step(2)
     w_out(-3)

time: 89.9 us -> 89.9 us (level)
  no operation moved by 1% of the time
where the time goes in v7:
time: 89.9 us; the launch traced here: 89.8 us
  Pallas kernels  86.7 us (96%)
  local copies, waits for them, and re-layouts  1.62 us (2%)
  other arithmetic  1.42 us (2%)
    pallas_call x1, Pallas kernels, local(): pl.pallas_call(kernel, out_shape=jax.ShapeDtypeStruct((T, 512), BF), in_s...  86.7 us

profile of v7, /device:TPU:1, one launch (start us, length us, event | category | flops | bytes accessed | tf_op | source)
XLA Modules:
  0.0 89.8 jit_solution(4559998351891682384)
XLA Ops:
  0.0 0.1 broadcast_multiply_fusion.1
  0.1 0.1 fusion.5
  0.2 0.6 pad_maximum_fusion.1.sn_ref
  0.8 0.6 pad_maximum_fusion.cs_ref
  1.4 86.7 %shard_map.118 = bf16[192,512]{1,0:T(8,128)(2,1)} custom-call(bf16[192,384]{1,0:T(8,128)(2,1)} %q_ref.1, bf16[192,512]{1,0:T(8,128)(2,1)} %lat_ref.1, bf16[32,192]{1,0:T(8,128)(2,1)} %bitcast.5, bf16[512,256]{1,0:T(8,128)(2,1)} %wk_ref.1, bf16[512,256]{1,0:T(8,128)(2,1)} %wv_ref.1, bf16[256,2048]{1,0:T(8,128)(2,1)} %wo_ref.1, bf16[192,512]{1,0:T(8,128)(2,1)} %res_ref.1, ...), custom_call_target="tpu_custom_call" | custom-call | tf_op jit(solution)/shard_map/pallas_call | solution.py:533
  88.2 1.6 %copy.14 = bf16[192,512]{1,0:T(8,128)(2,1)} copy(bf16[192,512]{1,0:T(8,128)(2,1)} %shard_map.118) | data formatting | bytes 393216
  (2 shorter events, 0.0 us)
